TPU v7x, 128 devices: a whole 4x4x4 slice. The times are simulated.
128 devices in a mesh: sp: 32 (over z, y, core), tp: 4 (over x).
Axes of the slice: x: 4, y: 4, z: 4, core: 2. Of those that a mesh axis runs over, the one named last changes fastest.
Arguments:
- tokens: bfloat16 [12288, 2048], P('sp', 'tp'), may hold values from -6 to 6
- norm_gain: float32 [2048], replicated, may hold values from 0.1 to 1.9
- w_query_down: bfloat16 [2048, 512], replicated, may hold values from -0.125 to 0.125
- query_gain: float32 [512], replicated, may hold values from 0.1 to 1.9
- w_query_up: bfloat16 [512, 1536], P(None, 'tp'), may hold values from -0.25 to 0.25
- w_latent_down: bfloat16 [2048, 256], replicated, may hold values from -0.125 to 0.125
- latent_gain: float32 [256], replicated, may hold values from 0.1 to 1.9
- w_rotary_key: bfloat16 [2048, 32], replicated, may hold values from -0.125 to 0.125
- w_latent_up: bfloat16 [256, 2048], P(None, 'tp'), may hold values from -0.375 to 0.375
- query_head_gain: float32 [96], replicated, may hold values from 0.1 to 1.9
- key_head_gain: float32 [96], replicated, may hold values from 0.1 to 1.9
- w_pool_in: bfloat16 [2048, 1024], P(None, 'tp'), may hold values from -0.125 to 0.125
- w_pool_mix: bfloat16 [4, 256, 256], P('tp'), may hold values from -0.375 to 0.375
- pool_scale: float32 [1024], P('tp'), may hold values from 0.1 to 1.9
- w_attn_out: bfloat16 [1024, 2048], P('tp'), may hold values from -12 to 12
- w_pool_out: bfloat16 [1024, 2048], P('tp'), may hold values from -0.5 to 0.5
- w_gate_attn: bfloat16 [2048, 2048], P(None, 'tp'), may hold values from -0.125 to 0.125
- w_gate_pool: bfloat16 [2048, 2048], P(None, 'tp'), may hold values from -0.125 to 0.125
Outputs:
- mixed: bfloat16 [12288, 2048], P('sp', 'tp')
All inputs are finite; a program needn't handle non-finite values.
Results may differ from a plain program's by a relative error of at most 0.02.
Values may be sent and summed in bfloat16 or wider, within the bound.
A program may use at most 128 MiB of HBM per device.

v0:
```python
import jax
import jax.numpy as jnp
from jax import lax
from jax.sharding import PartitionSpec as P

NOPE = 64
ROPE = 32
VALUE_DIM = 64
POOL_GROUPS = 4
POOL_GROUP = 256


eps = 1e-06
theta = 10000.0


def sent_to_all(value, axis):
    copies = jnp.broadcast_to(value, (lax.axis_size(axis), *value.shape))
    return lax.all_to_all(copies, axis, split_axis=0, concat_axis=0, tiled=True)


def in_order(parts, dim):
    lengths = list(parts.shape[1:])
    lengths[dim] *= parts.shape[0]
    return jnp.moveaxis(parts, 0, dim).reshape(lengths)


def gathered_copies(value, axis, dim):
    parts = sent_to_all(value, axis)
    return in_order(parts, dim)


def side_by_side(arrays, axis, dim, along):
    ends, at = ([], 0)
    for a in arrays[:-1]:
        at += a.shape[along]
        ends.append(at)
    both = jnp.concatenate(arrays, axis=along)
    return tuple(jnp.split(lax.all_gather(both, axis, axis=dim, tiled=True), ends, axis=along))


def extended(cells, sides, width):
    for axis, dim in sides:
        count = lax.axis_size(axis)
        ends = count - 1
        head = lax.slice_in_dim(cells, 0, width, axis=dim)
        tail = lax.slice_in_dim(cells, cells.shape[dim] - width, cells.shape[dim], axis=dim)
        cells = jnp.concatenate(
            [
                lax.ppermute(tail, axis, [(i, (i + 1) % count) for i in range(ends)]),
                cells,
                lax.ppermute(head, axis, [((i + 1) % count, i) for i in range(ends)]),
            ],
            axis=dim,
        )
    return cells


def in_one_piece(arrays, axis, dim, along):
    both = jnp.concatenate(arrays, axis=along)
    out, at, outs = (gathered_copies(both, axis, dim), 0, [])
    for a in arrays:
        outs.append(lax.slice_in_dim(out, at, at + a.shape[along], axis=along))
        at += a.shape[along]
    return tuple(outs)


def rms_scale(values, gain):
    values = values.astype(jnp.float32)
    return values * lax.rsqrt(jnp.mean(values * values, axis=-1, keepdims=True) + eps) * gain


def rotate(values, positions):
    half = values.shape[-1] // 2
    freqs = theta ** (-jnp.arange(half, dtype=jnp.float32) / half)
    angles = positions.astype(jnp.float32)[:, None] * freqs[None, :]
    cosine = jnp.cos(angles)[:, None, :]
    sine = jnp.sin(angles)[:, None, :]
    first = values[..., :half]
    second = values[..., half:]
    return jnp.concatenate(
        [first * cosine - second * sine, first * sine + second * cosine], axis=-1
    )


def head_finish(values, gain, positions):
    normed = rms_scale(values, gain)
    return jnp.concatenate([normed[..., :NOPE], rotate(normed[..., NOPE:], positions)], axis=-1)


def body(
    tokens,
    norm_gain,
    w_query_down,
    query_gain,
    w_query_up,
    w_latent_down,
    latent_gain,
    w_rotary_key,
    w_latent_up,
    query_head_gain,
    key_head_gain,
    w_pool_in,
    w_pool_mix,
    pool_scale,
    w_attn_out,
    w_pool_out,
    w_gate_attn,
    w_gate_pool,
):
    bf = jnp.bfloat16
    rows = tokens.shape[0]
    length = rows * lax.axis_size("sp")
    local_heads = w_query_up.shape[1] // (NOPE + ROPE)
    positions = lax.axis_index("sp") * rows + jnp.arange(rows, dtype=jnp.int32)
    whole = gathered_copies(tokens, "tp", 1)
    normed = rms_scale(whole, norm_gain).astype(bf)
    query_latent = jnp.dot(normed, w_query_down, preferred_element_type=jnp.float32).astype(bf)
    query_normed = rms_scale(query_latent, query_gain).astype(bf)
    query_raw = jnp.dot(query_normed, w_query_up, preferred_element_type=jnp.float32).astype(bf)
    query_raw = query_raw.reshape(rows, local_heads, NOPE + ROPE)
    query = (head_finish(query_raw, query_head_gain, positions) * (NOPE + ROPE) ** (-0.5)).astype(
        bf
    )
    latent = jnp.dot(normed, w_latent_down, preferred_element_type=jnp.float32).astype(bf)
    key_latent = rms_scale(latent, latent_gain).astype(bf)
    rotary_key = jnp.dot(normed, w_rotary_key, preferred_element_type=jnp.float32).astype(bf)
    start_state = (
        jnp.full((local_heads, rows), -1e30, jnp.float32),
        jnp.zeros((local_heads, rows), jnp.float32),
        jnp.zeros((local_heads, rows, VALUE_DIM), jnp.float32),
    )
    latent_piece, rotary_piece = side_by_side((key_latent, rotary_key), "sp", 0, 1)
    blocks = latent_piece.shape[0] // rows
    latent_blocks = latent_piece.reshape(blocks, rows, latent_piece.shape[1])
    rotary_blocks = rotary_piece.reshape(blocks, rows, rotary_piece.shape[1])

    def one_block(state, items):
        latent_block, rotary_block, number = items
        top, total, summed = state
        key_positions = number * rows + jnp.arange(rows, dtype=jnp.int32)
        keys_values = jnp.dot(latent_block, w_latent_up, preferred_element_type=jnp.float32).astype(
            bf
        )
        keys_values = keys_values.reshape(rows, local_heads, NOPE + VALUE_DIM)
        key_raw = jnp.concatenate(
            [
                keys_values[..., :NOPE],
                jnp.broadcast_to(rotary_block[:, None, :], (rows, local_heads, ROPE)),
            ],
            axis=-1,
        )
        key = head_finish(key_raw, key_head_gain, key_positions).astype(bf)
        values = keys_values[..., NOPE:]
        scores = jnp.einsum("qhd,khd->hqk", query, key, preferred_element_type=jnp.float32)
        new_top = jnp.maximum(top, jnp.max(scores, axis=-1))
        factor = jnp.exp(top - new_top)
        expo = jnp.exp(scores - new_top[..., None])
        total = total * factor + jnp.sum(expo, axis=-1)
        summed = summed * factor[..., None] + jnp.einsum(
            "hqk,khv->hqv", expo.astype(bf), values, preferred_element_type=jnp.float32
        )
        return ((new_top, total, summed), None)

    state, _ = lax.scan(
        one_block, start_state, (latent_blocks, rotary_blocks, jnp.arange(blocks, dtype=jnp.int32))
    )
    top, total, summed = state
    attn_rows = jnp.transpose(summed / total[..., None], (1, 0, 2)).reshape(
        rows, local_heads * VALUE_DIM
    )
    attn_rows = attn_rows.astype(bf)
    pool_input = jnp.dot(normed, w_pool_in, preferred_element_type=jnp.float32).astype(bf)
    reach = 2**POOL_GROUPS // 2
    padded = extended(pool_input, (("sp", 0),), reach).astype(jnp.float32)
    local_groups = w_pool_mix.shape[0]
    group_ids = lax.axis_index("tp") * local_groups + jnp.arange(local_groups, dtype=jnp.int32)
    windows = jnp.power(2, group_ids + 1)
    channel_window = jnp.repeat(windows, POOL_GROUP)
    pooled = jnp.zeros((rows, local_groups * POOL_GROUP), jnp.float32)
    for shift in range(-reach, reach):
        inside = (shift >= -(channel_window // 2)) & (
            shift <= channel_window - channel_window // 2 - 1
        )
        pooled = pooled + jnp.where(
            inside[None, :], padded[reach + shift : reach + shift + rows], 0.0
        )
    low = jnp.clip(positions[:, None] - channel_window[None, :] // 2, 0, length)
    high = jnp.clip(
        positions[:, None] + channel_window[None, :] - channel_window[None, :] // 2, 0, length
    )
    count = (high - low).astype(jnp.float32)
    pool_mixed = (pooled / count - pool_input.astype(jnp.float32)).astype(bf)
    pool_mixed = pool_mixed.reshape(rows, local_groups, POOL_GROUP)
    grouped = jnp.einsum("lgc,gcd->lgd", pool_mixed, w_pool_mix, preferred_element_type=jnp.float32)
    pool_rows = (grouped.reshape(rows, local_groups * POOL_GROUP) * pool_scale).astype(bf)
    gate_attn = jax.nn.sigmoid(jnp.dot(normed, w_gate_attn, preferred_element_type=jnp.float32))
    gate_pool = jax.nn.sigmoid(jnp.dot(normed, w_gate_pool, preferred_element_type=jnp.float32))
    attn_tokens, pool_tokens = (
        lax.all_to_all(attn_rows, "tp", split_axis=0, concat_axis=1, tiled=True),
        lax.all_to_all(pool_rows, "tp", split_axis=0, concat_axis=1, tiled=True),
    )
    attn_weight, pool_weight = in_one_piece((w_attn_out, w_pool_out), "tp", 0, 1)
    attn_here = jnp.dot(attn_tokens, attn_weight, preferred_element_type=jnp.float32)
    pool_here = jnp.dot(pool_tokens, pool_weight, preferred_element_type=jnp.float32)
    attn_branch, pool_branch = (
        lax.all_to_all(
            attn_here.astype(jnp.bfloat16), "tp", split_axis=1, concat_axis=0, tiled=True
        ).astype(attn_here.dtype),
        lax.all_to_all(
            pool_here.astype(jnp.bfloat16), "tp", split_axis=1, concat_axis=0, tiled=True
        ).astype(pool_here.dtype),
    )
    return (gate_attn * attn_branch + gate_pool * pool_branch).astype(bf)


def solution(mesh):
    placed = (
        P("sp", "tp"),
        P(),
        P(),
        P(),
        P(None, "tp"),
        P(),
        P(),
        P(),
        P(None, "tp"),
        P(),
        P(),
        P(None, "tp"),
        P("tp", None, None),
        P("tp"),
        P("tp", None),
        P("tp", None),
        P(None, "tp"),
        P(None, "tp"),
    )
    return jax.shard_map(body, mesh=mesh, in_specs=placed, out_specs=P("sp", "tp"), check_vma=False)
```

profile of v0, /device:TPU:0, one launch (start us, length us, event | category | flops | bytes accessed | tf_op | source)
XLA Modules:
  0.0 303.7 jit_solution(15979161657905647551)
XLA Ops:
  6.5 1.4 copy.39
  8.1 24.9 %all_to_all.68 = bf16[4,384,512]{1,2,0:T(8,128)(2,1)S(1)} all-to-all(bf16[4,384,512]{1,2,0:T(8,128)(2,1)S(1)} %broadcast_in_dim.172), channel_id=1, replica_groups=mesh['sp'=32,'tp'=4] {'tp'}, dimensions={0} | all-to-all | bytes 3145728 | tf_op jit(solution)/shard_map/all_to_all | solution.py:19
  37.4 2.9 pad_maximum_fusion.1
  40.9 1.3 collective-permute-start
  42.3 1.4 collective-permute-start.1
  45.6 1.7 collective-permute-done.1
  47.3 1.4 fusion.67
  49.4 3.4 %all-to-all-start.4 = ((bf16[4,96,256]{2,1,0:T(8,128)(2,1)}), bf16[4,96,256]{2,1,0:T(8,128)(2,1)S(1)}, u32[]{:S(2)}, u32[]{:S(2)}) async-start(bf16[4,96,256]{2,1,0:T(8,128)(2,1)} %multiply_convert_fusion.2), calls=%async_computation.4 | async-start | bytes 393216 | tf_op jit(solution)/shard_map/all_to_all | solution.py:201
  53.0 6.1 %all-to-all-done.4 = bf16[4,96,256]{2,1,0:T(8,128)(2,1)S(1)} async-done(((bf16[4,96,256]{2,1,0:T(8,128)(2,1)}), bf16[4,96,256]{2,1,0:T(8,128)(2,1)S(1)}, u32[]{:S(2)}, u32[]{:S(2)}) %all-to-all-start.4) | async-done | bytes 196640 | tf_op jit(solution)/shard_map/all_to_all | solution.py:201
  59.1 5.9 %broadcast_in_dim.176 = bf16[4,256,4096]{2,1,0:T(8,128)(2,1)} broadcast(bf16[256,4096]{1,0:T(8,128)(2,1)} %pad_maximum_fusion.1), dimensions={1,2} | broadcast | bytes 10485760 | tf_op jit(solution)/shard_map/broadcast_in_dim | solution.py:18
  65.0 5.7 %all-to-all-start.2 = ((bf16[4,256,4096]{2,1,0:T(8,128)(2,1)}), bf16[4,256,4096]{2,1,0:T(8,128)(2,1)}, u32[]{:S(2)}, u32[]{:S(2)}) async-start(bf16[4,256,4096]{2,1,0:T(8,128)(2,1)} %broadcast_in_dim.176), calls=%async_computation.2 | async-start | bytes 16777216 | tf_op jit(solution)/shard_map/all_to_all | solution.py:19
  70.7 22.1 %all-gather.2.cloned.1.call-done = bf16[12288,288]{0,1:T(8,128)(2,1)} async-done(((bf16[384,288]{0,1:T(8,128)(2,1)}), bf16[12288,288]{0,1:T(8,128)(2,1)}) %all-gather.2.cloned.1.call-update) | async-done | bytes 7077904 | tf_op jit(solution)/shard_map/all_gather | solution.py:39
  92.7 6.0 %split.8 = bf16[12288,256]{0,1:T(8,128)(2,1)} slice(bf16[12288,288]{0,1:T(8,128)(2,1)} %all-gather.2.cloned.1.call-done), slice={[0:12288], [0:256]} | slice | bytes 12582912 | tf_op jit(solution)/shard_map/split | solution.py:39
  98.8 8.7 %copy.48 = bf16[12288,256]{1,0:T(8,128)(2,1)} copy(bf16[12288,256]{0,1:T(8,128)(2,1)} %split.8) | data formatting | bytes 12582912
  108.7 149.8 %while.15 = (s32[]{:T(128)}, f32[4,384]{1,0:T(4,128)S(1)}, f32[4,384]{1,0:T(4,128)S(1)}, f32[4,384,64]{1,2,0:T(8,128)S(1)}, bf16[32,384,256]{2,1,0:T(8,128)(2,1)...) while((s32[]{:T(128)}, f32[4,384]{1,0:T(4,128)S(1)}, ...), condition=%wide.region_8.9_spmd.clone, body=%wide.region_4.8_spmd.clone.sunk | while | flops 295714592 | bytes 12947125 | solution.py:165
  114.9 1.2 convolution_convert_fusion.7
  119.6 1.2 convolution_convert_fusion.7
  124.3 1.2 convolution_convert_fusion.7
  129.0 1.2 convolution_convert_fusion.7
  133.6 1.2 convolution_convert_fusion.7
  138.3 1.2 convolution_convert_fusion.7
  143.0 1.2 convolution_convert_fusion.7
  147.7 1.2 convolution_convert_fusion.7
  152.4 1.2 convolution_convert_fusion.7
  157.1 1.2 convolution_convert_fusion.7
  161.7 1.2 convolution_convert_fusion.7
  166.4 1.2 convolution_convert_fusion.7
  171.1 1.2 convolution_convert_fusion.7
  175.8 1.2 convolution_convert_fusion.7
  180.5 1.2 convolution_convert_fusion.7
  185.1 1.2 convolution_convert_fusion.7
  189.8 1.2 convolution_convert_fusion.7
  194.5 1.2 convolution_convert_fusion.7
  199.2 1.2 convolution_convert_fusion.7
  203.9 1.2 convolution_convert_fusion.7
  213.2 1.2 convolution_convert_fusion.7
  232.0 1.2 convolution_convert_fusion.7
  250.7 1.2 convolution_convert_fusion.7
  259.7 4.2 %all-to-all-start.1 = ((bf16[4,96,256]{2,1,0:T(8,128)(2,1)}), bf16[4,96,256]{2,1,0:T(8,128)(2,1)S(1)}, u32[]{:S(2)}, u32[]{:S(2)}) async-start(bf16[4,96,256]{2,1,0:T(8,128)(2,1)} %copy.42), calls=%async_computation.1 | async-start | bytes 393216 | tf_op jit(solution)/shard_map/all_to_all | solution.py:200
  263.9 3.0 fusion.28
  267.7 2.6 all-to-all-done.1
  270.3 3.5 %all-to-all-start.5 = ((bf16[96,4,512]{2,0,1:T(8,128)(2,1)}), bf16[96,4,512]{2,0,1:T(8,128)(2,1)S(1)}, u32[]{:S(2)}, u32[]{:S(2)}) async-start(bf16[96,4,512]{2,0,1:T(8,128)(2,1)} %bitcast.106), calls=%async_computation.5 | async-start | bytes 786432 | tf_op jit(solution)/shard_map/all_to_all | solution.py:210
  273.8 3.0 fusion.25
  277.6 3.5 %all-to-all-done.5 = bf16[96,4,512]{2,0,1:T(8,128)(2,1)S(1)} async-done(((bf16[96,4,512]{2,0,1:T(8,128)(2,1)}), bf16[96,4,512]{2,0,1:T(8,128)(2,1)S(1)}, u32[]{:S(2)}, u32[]{:S(2)}) %all-to-all-start.5) | async-done | bytes 393248 | tf_op jit(solution)/shard_map/all_to_all | solution.py:210
  281.1 3.5 %all-to-all-start.3 = ((bf16[96,4,512]{2,0,1:T(8,128)(2,1)}), bf16[96,4,512]{2,0,1:T(8,128)(2,1)S(1)}, u32[]{:S(2)}, u32[]{:S(2)}) async-start(bf16[96,4,512]{2,0,1:T(8,128)(2,1)} %bitcast.107), calls=%async_computation.3 | async-start | bytes 786432 | tf_op jit(solution)/shard_map/all_to_all | solution.py:207
  284.7 7.3 %all-to-all-done.3 = bf16[96,4,512]{2,0,1:T(8,128)(2,1)S(1)} async-done(((bf16[96,4,512]{2,0,1:T(8,128)(2,1)}), bf16[96,4,512]{2,0,1:T(8,128)(2,1)S(1)}, u32[]{:S(2)}, u32[]{:S(2)}) %all-to-all-start.3) | async-done | bytes 393248 | tf_op jit(solution)/shard_map/all_to_all | solution.py:207
  292.0 2.9 fusion.35
  294.9 1.9 fusion.40
  (707 shorter events, 109.0 us)
Async XLA Ops:
  6.5 37.2 %copy-start = (bf16[2048,512]{1,0:T(8,128)(2,1)S(1)}, bf16[2048,512]{1,0:T(8,128)(2,1)}, u32[]{:S(2)}) copy-start(bf16[2048,512]{1,0:T(8,128)(2,1)} %param.22) | copy-start | bytes 6291460
  6.5 86.2 %all-gather.2.cloned.1.call-start = ((), (), s32[]{:S(2)}) async-start(), calls=%async_computation.6 | async-start | bytes 7299072 | tf_op jit(solution)/shard_map/all_gather | solution.py:39
  8.0 25.4 %copy-start.14 = (f32[2048]{0:T(1024)S(1)}, f32[2048]{0:T(1024)}, u32[]{:S(2)}) copy-start(f32[2048]{0:T(1024)} %param.21) | copy-start | bytes 24580
  33.0 0.9 copy-start.10
  33.4 1.2 copy-start.20
  33.9 1.6 copy-start.2
  34.6 0.8 copy-start.16
  34.7 2.7 copy-start.7
  37.4 2.9 copy-start.3
  37.4 2.9 copy-start.8
  40.9 4.6 %collective-permute-start = (bf16[8,256]{1,0:T(8,128)(2,1)S(1)}, bf16[8,256]{1,0:T(8,128)(2,1)S(1)}, u32[]{:S(2)}, u32[]{:S(2)}) collective-permute-start(bf16[8,256]{1,0:T(8,128)(2,1)S(1)} %get-tuple-element.153), channel_id=1, source_target_pairs={{0,4},{4,8},{8,12},{12,16},{16,20},{20,24},{24,28},{28,32},{32,36}... | collective-permute-start | bytes 12296 | tf_op jit(solution)/shard_map/ppermute | solution.py:50
  42.2 2.6 copy-start.9
  42.2 2.6 copy-start.15
  42.2 3.2 %copy-start.18 = (f32[96]{0:T(128)S(1)}, f32[96]{0:T(128)}, u32[]{:S(2)}) copy-start(f32[96]{0:T(128)} %param.29) | copy-start | bytes 1156
  42.3 5.0 %collective-permute-start.1 = (bf16[8,256]{1,0:T(8,128)(2,1)S(1)}, bf16[8,256]{1,0:T(8,128)(2,1)S(1)}, u32[]{:S(2)}, u32[]{:S(2)}) collective-permute-start(bf16[8,256]{1,0:T(8,128)(2,1)S(1)} %get-tuple-element.154), channel_id=1, source_target_pairs={{4,0},{8,4},{12,8},{16,12},{20,16},{24,20},{28,24},{32,28},{36,32}... | collective-permute-start | bytes 12296 | tf_op jit(solution)/shard_map/ppermute | solution.py:52
  44.8 2.5 copy-start.21
  47.3 1.4 copy-start.17
  47.3 5.5 %copy-start.11 = (f32[384,16]{0,1:T(8,128)S(1)}, f32[384,16]{0,1:T(8,128)}, u32[]{:S(2)}) copy-start(f32[384,16]{0,1:T(8,128)} %get-tuple-element.155) | copy-start | bytes 73732
  47.3 5.5 %copy-start.12 = (f32[384,16]{0,1:T(8,128)S(1)}, f32[384,16]{0,1:T(8,128)}, u32[]{:S(2)}) copy-start(f32[384,16]{0,1:T(8,128)} %get-tuple-element.156) | copy-start | bytes 73732
  49.4 9.7 %all-to-all-start.4 = ((bf16[4,96,256]{2,1,0:T(8,128)(2,1)}), bf16[4,96,256]{2,1,0:T(8,128)(2,1)S(1)}, u32[]{:S(2)}, u32[]{:S(2)}) async-start(bf16[4,96,256]{2,1,0:T(8,128)(2,1)} %multiply_convert_fusion.2), calls=%async_computation.4 | async-start | bytes 393216 | tf_op jit(solution)/shard_map/all_to_all | solution.py:201
  65.0 194.7 %all-to-all-start.2 = ((bf16[4,256,4096]{2,1,0:T(8,128)(2,1)}), bf16[4,256,4096]{2,1,0:T(8,128)(2,1)}, u32[]{:S(2)}, u32[]{:S(2)}) async-start(bf16[4,256,4096]{2,1,0:T(8,128)(2,1)} %broadcast_in_dim.176), calls=%async_computation.2 | async-start | bytes 16777216 | tf_op jit(solution)/shard_map/all_to_all | solution.py:19
  107.5 1.1 slice-start
  107.5 1.2 copy-start.6
  107.5 1.2 copy-start.13
  259.7 10.6 %all-to-all-start.1 = ((bf16[4,96,256]{2,1,0:T(8,128)(2,1)}), bf16[4,96,256]{2,1,0:T(8,128)(2,1)S(1)}, u32[]{:S(2)}, u32[]{:S(2)}) async-start(bf16[4,96,256]{2,1,0:T(8,128)(2,1)} %copy.42), calls=%async_computation.1 | async-start | bytes 393216 | tf_op jit(solution)/shard_map/all_to_all | solution.py:200
  270.3 10.8 %all-to-all-start.5 = ((bf16[96,4,512]{2,0,1:T(8,128)(2,1)}), bf16[96,4,512]{2,0,1:T(8,128)(2,1)S(1)}, u32[]{:S(2)}, u32[]{:S(2)}) async-start(bf16[96,4,512]{2,0,1:T(8,128)(2,1)} %bitcast.106), calls=%async_computation.5 | async-start | bytes 786432 | tf_op jit(solution)/shard_map/all_to_all | solution.py:210
  276.8 15.2 %copy-start.4 = (bf16[384,2048]{0,1:T(8,128)(2,1)S(1)}, bf16[384,2048]{0,1:T(8,128)(2,1)}, u32[]{:S(2)}) copy-start(bf16[384,2048]{0,1:T(8,128)(2,1)} %copy-done.2) | copy-start | bytes 4718596
  281.1 10.8 %all-to-all-start.3 = ((bf16[96,4,512]{2,0,1:T(8,128)(2,1)}), bf16[96,4,512]{2,0,1:T(8,128)(2,1)S(1)}, u32[]{:S(2)}, u32[]{:S(2)}) async-start(bf16[96,4,512]{2,0,1:T(8,128)(2,1)} %bitcast.107), calls=%async_computation.3 | async-start | bytes 786432 | tf_op jit(solution)/shard_map/all_to_all | solution.py:207
  292.0 2.9 copy-start.5
  292.0 2.9 copy-start.19
  294.9 1.9 copy-start.1
Sparse Core Ops, SparseCore 0:
  36.4 56.2 all-gather.1
where the time goes:
time: 306 us; the launch traced here: 304 us
  matrix products  87.7 us (29%)
  local copies, waits for them, and re-layouts  54.4 us (18%)
  waiting for transfers between devices  43.3 us (14%)
  other arithmetic  31.3 us (10%)
  loops' own time  25.1 us (8%)
  blocking collectives  24.9 us (8%)
  starting transfers between devices  22.9 us (7%)
  between operations  14.1 us (5%)
    dot_general x32, matrix products, one_block(): jnp.dot(latent_block, w_latent_up, preferred_element_type=jnp.float32)  38.1 us
    another operation x1, loops' own time, body(): lax.scan(one_block, start_state, (latent_blocks, rotary_blocks, jnp.arang...  25.1 us
    all_to_all x1, blocking collectives, sent_to_all(): return lax.all_to_all(copies, axis, split_axis=0, concat_axis=0, tiled=True)  24.9 us
    all_gather x1, waiting for transfers between devices, side_by_side(): lax.all_gather(both, axis, axis=dim, tiled=True)  22.1 us
    dynamic_slice x32, local copies, waits for them, and re-layouts, body(): lax.scan(one_block, start_state, (latent_blocks, rotary_blocks, jnp.arang...  18.8 us
    dot_general x32, matrix products, one_block(): jnp.einsum('hqk,khv->hqv', expo.astype(bf), values, preferred_element_typ...  17.1 us
    dot_general x32, matrix products, one_block(): jnp.einsum('qhd,khd->hqk', query, key, preferred_element_type=jnp.float32)  17 us
    reduce_sum x32, other arithmetic, one_block(): total = total * factor + jnp.sum(expo, axis=-1)  10.7 us
  transfers between devices with their start and end apart: 8, of which 6 were waited for; matrix products, arithmetic and copies ran while one was open for 54% of the time, Pallas kernels for 0%

commit v1 on v0

v1 whole, which is shorter than its diff:
```python
import functools
import numpy as np
import jax
import jax.numpy as jnp
from jax import lax
from jax.experimental import pallas as pl
from jax.experimental.pallas import tpu as pltpu
from jax.sharding import PartitionSpec as P

NOPE = 64
ROPE = 32
HEAD = NOPE + ROPE
VALUE_DIM = 64
POOL_GROUPS = 4
POOL_GROUP = 256
ROWS = 384
HEADS_HERE = 4
LATENT = 256
KEY_ROWS = 304
CHUNK = 128
MESH = pl.DeviceIdType.MESH

eps = 1e-06
theta = 10000.0
LOG2E = 1.4426950408889634
bf = jnp.bfloat16
f32 = jnp.float32


def rope_tables():
    half = ROPE // 2
    freqs = theta ** (-np.arange(half, dtype=np.float64) / half)
    fine = np.arange(ROWS)[None, :] * freqs[:, None]
    coarse = (np.arange(128) * ROWS)[None, :] * freqs[:, None]
    fine = np.stack([np.cos(fine), np.sin(fine)]).astype(np.float32)
    coarse = np.stack([np.cos(coarse), np.sin(coarse)]).astype(np.float32)
    return fine, coarse


def column(row):
    wide = jnp.concatenate([row, jnp.zeros((1, 128 - row.shape[1]), f32)], axis=1)
    return jnp.broadcast_to(wide, (128, 128)).T


def front_kernel(
    tok, ng, wq_h, qg, wu_h, wl_h, lg, wr_h, qhg, khg, fine, coarse,
    normed, block, q_out,
    whole, wq, wu, wl, wr, wsem, s_r, r_r, s_l, r_l, s_fr, r_fr, s_fl, r_fl,
):
    sp = lax.axis_index("sp")
    me = lax.axis_index("tp")
    right, left = (me + 1) % 4, (me + 3) % 4
    loads = [
        pltpu.make_async_copy(src, dst, wsem.at[i])
        for i, (src, dst) in enumerate(((wl_h, wl), (wr_h, wr), (wq_h, wq), (wu_h, wu)))
    ]
    for load in loads:
        load.start()
    barrier = pltpu.get_barrier_semaphore()
    for peer in (left, right):
        pl.semaphore_signal(barrier, inc=1, device_id=(sp, peer), device_id_type=MESH)
    pl.semaphore_wait(barrier, 2)

    def rows_of(c, off=0, n=CHUNK):
        return pl.ds(pl.multiple_of(c * CHUNK + off, 16), n)

    def own(c, to, send, recv):
        return pltpu.make_async_remote_copy(
            src_ref=tok.at[rows_of(c)], dst_ref=whole.at[me, rows_of(c)],
            send_sem=send.at[c], recv_sem=recv.at[c], device_id=(sp, to), device_id_type=MESH,
        )

    def relay(c, owner, off, to, send, recv):
        part = whole.at[owner, rows_of(c, off, CHUNK // 2)]
        return pltpu.make_async_remote_copy(
            src_ref=part, dst_ref=part,
            send_sem=send.at[c], recv_sem=recv.at[c], device_id=(sp, to), device_id_type=MESH,
        )

    def rightward(c):
        return own(c, right, s_r, r_r)

    def leftward(c):
        return own(c, left, s_l, r_l)

    def relay_right(c):
        return relay(c, left, 0, right, s_fr, r_fr)

    def relay_left(c):
        return relay(c, right, CHUNK // 2, left, s_fl, r_fl)

    for c in range(2):
        rightward(c).start()
        leftward(c).start()
    whole[me] = tok[...]
    rightward(0).wait_recv()
    relay_right(0).start()
    leftward(0).wait_recv()
    relay_left(0).start()
    rightward(2).start()
    leftward(2).start()

    pick = lax.broadcasted_iota(jnp.int32, (16, 128), 1) == sp
    cc = jnp.sum(jnp.where(pick, coarse[0], 0.0), axis=1, keepdims=True)
    cs = jnp.sum(jnp.where(pick, coarse[1], 0.0), axis=1, keepdims=True)
    q_gain = column(qhg[...])
    k_gain = column(khg[...])
    for load in loads:
        load.wait()

    def step(c, carry):
        @pl.when(c < 2)
        def _():
            rightward(c + 1).wait_recv()
            relay_right(c + 1).start()
            leftward(c + 1).wait_recv()
            relay_left(c + 1).start()

        relay_right(c).wait_recv()
        relay_left(c).wait_recv()
        rows = rows_of(c)
        lanes = pl.ds(pl.multiple_of(c * CHUNK, 128), CHUNK)
        squares = jnp.zeros((CHUNK, 1), f32)
        for k in range(4):
            v = whole[k, rows].astype(f32)
            squares = squares + jnp.sum(v * v, axis=1, keepdims=True)
        scale = lax.rsqrt(squares * (1.0 / 2048) + eps)
        for k in range(4):
            v = whole[k, rows].astype(f32)
            normed[rows, k * 512 : (k + 1) * 512] = (
                v * scale * ng[:, k * 512 : (k + 1) * 512]
            ).astype(bf)
        here = normed[rows, :]
        lat = jnp.dot(here, wl[...], preferred_element_type=f32).astype(bf).astype(f32)
        lat = lat * lax.rsqrt(jnp.mean(lat * lat, axis=1, keepdims=True) + eps) * lg[...]
        block[0:LATENT, lanes] = lat.T.astype(bf)
        fc, fs = fine[0, :, lanes], fine[1, :, lanes]
        cosine = cc * fc - cs * fs
        sine = cs * fc + cc * fs

        def rotated(first, second):
            return first * cosine - second * sine, first * sine + second * cosine

        rot = jnp.dot(here, wr[...], preferred_element_type=f32).astype(bf).astype(f32)
        rot = jnp.concatenate([rot, jnp.zeros((CHUNK, 96), f32)], axis=1).T[0:ROPE]
        total = jnp.sum(rot * rot, axis=0, keepdims=True)
        high = total.astype(bf).astype(f32)
        low = total - high
        rot = rot * k_gain[NOPE:HEAD]
        first, second = rotated(rot[0:16], rot[16:32])
        line = lax.broadcasted_iota(jnp.int32, (16, CHUNK), 0)
        tail = jnp.where(line == 0, high, jnp.where(line == 1, low, 0.0))
        block[256:272, lanes] = first.astype(bf)
        block[272:288, lanes] = second.astype(bf)
        block[288:304, lanes] = tail.astype(bf)

        lat = jnp.dot(here, wq[...], preferred_element_type=f32).astype(bf).astype(f32)
        lat = lat * lax.rsqrt(jnp.mean(lat * lat, axis=1, keepdims=True) + eps) * qg[...]
        raw = jnp.dot(lat.astype(bf), wu[...], preferred_element_type=f32)
        raw = raw.astype(bf).astype(f32).T
        for h in range(HEADS_HERE):
            v = raw[h * HEAD : (h + 1) * HEAD]
            r = lax.rsqrt(jnp.mean(v * v, axis=0, keepdims=True) + eps)
            v = v * (r * (HEAD ** (-0.5) * LOG2E)) * q_gain[0:HEAD]
            first, second = rotated(v[64:80], v[80:96])
            v = jnp.concatenate(
                [v[0:NOPE] * k_gain[0:NOPE], first, second, jnp.zeros((32, CHUNK), f32)], axis=0
            )
            q_out[h, rows, :] = v.T.astype(bf)
        return carry

    lax.fori_loop(0, 3, step, 0)
    for c in range(3):
        for copy in (rightward(c), leftward(c), relay_right(c), relay_left(c)):
            copy.wait_send()


def front(tokens, norm_gain, wq, qg, wu, wl, lg, wr, qhg, khg):
    fine, coarse = rope_tables()
    vmem = pl.BlockSpec(memory_space=pltpu.VMEM)
    hbm = pl.BlockSpec(memory_space=pl.ANY)
    sems = pltpu.SemaphoreType.DMA((3,))
    return pl.pallas_call(
        front_kernel,
        out_shape=(
            jax.ShapeDtypeStruct((ROWS, 2048), bf),
            jax.ShapeDtypeStruct((KEY_ROWS, ROWS), bf),
            jax.ShapeDtypeStruct((HEADS_HERE, ROWS, 128), bf),
        ),
        in_specs=[vmem, vmem, hbm, vmem, hbm, hbm, vmem, hbm, vmem, vmem, vmem, vmem],
        out_specs=(vmem, vmem, vmem),
        scratch_shapes=[
            pltpu.VMEM((4, ROWS, 512), bf),
            pltpu.VMEM((2048, 512), bf),
            pltpu.VMEM((512, 384), bf),
            pltpu.VMEM((2048, 256), bf),
            pltpu.VMEM((2048, 32), bf),
            pltpu.SemaphoreType.DMA((4,)),
        ]
        + [sems] * 8,
        compiler_params=pltpu.CompilerParams(
            collective_id=0, has_side_effects=True, vmem_limit_bytes=40 * 2**20
        ),
        name="front",
    )(
        tokens, norm_gain.reshape(1, -1), wq, qg.reshape(1, -1), wu, wl, lg.reshape(1, -1), wr,
        qhg.reshape(1, -1), khg.reshape(1, -1), fine, coarse,
    )


ORDER = (
    (0, 0),
    (3, 0), (1, 0), (0, 3), (0, 1),
    (2, 0), (0, 2),
    (3, 3), (3, 1), (1, 3), (1, 1),
    (3, 2), (1, 2), (2, 3), (2, 1),
    (2, 2),
)
EVENTS = (1, 3, 6, 9, 11)
HALVES = ((0, 160), (160, 144))
PARTS = (((0, 80), (80, 80)), ((160, 80), (240, 64)))
STEPS = (1, 3)


def attend_kernel(
    q, block, w_up, out, g, acc, kt, vt, wt,
    s_own, r_own, s_1f, r_1f, s_1h, r_1h, s_2f, r_2f, s_2h, r_2h, s_d, r_d,
):
    sp = lax.axis_index("sp")
    tp = lax.axis_index("tp")
    core, y, z = sp % 2, (sp // 2) % 4, sp // 8
    partner = sp + 1 - 2 * core
    lanes = pl.ds(pl.multiple_of(core * ROWS, 128), ROWS)

    def slot(dy, dz):
        return ((z + dz) % 4) * 4 + (y + dy) % 4

    def device(dy, dz):
        return (slot(dy, dz) * 2 + core, tp)

    def offsets(half, along, across):
        return (along, across) if half == 0 else (across, along)

    def region(off, rows):
        return g.at[slot(*off), pl.ds(rows[0], rows[1]), lanes]

    def copy(src, dst, to, send, recv):
        return pltpu.make_async_remote_copy(
            src_ref=src, dst_ref=dst, send_sem=send, recv_sem=recv,
            device_id=to, device_id_type=MESH,
        )

    def mine(rows):
        return block.at[pl.ds(rows[0], rows[1]), :]

    def first_full(half, d):
        rows = HALVES[half]
        return copy(
            mine(rows), region((0, 0), rows), device(*offsets(half, STEPS[d], 0)),
            s_1f.at[half, d], r_1f.at[half, d],
        )

    def first_part(half, d):
        part = region(offsets(half, STEPS[1 - d], 0), PARTS[half][d])
        return copy(
            part, part, device(*offsets(half, STEPS[d], 0)),
            s_1h.at[half, d], r_1h.at[half, d],
        )

    def second_full(half, along, d):
        rows = HALVES[half]
        part = region(offsets(half, along, 0), rows)
        return copy(
            mine(rows) if along == 0 else part, part, device(*offsets(half, 0, STEPS[d])),
            s_2f.at[half, along, d], r_2f.at[half, along, d],
        )

    def second_part(half, along, d):
        part = region(offsets(half, along, STEPS[1 - d]), PARTS[half][d])
        return copy(
            part, part, device(*offsets(half, 0, STEPS[d])),
            s_2h.at[half, along, d], r_2h.at[half, along, d],
        )

    def across_chip(half, off):
        part = region(off, HALVES[half])
        at = off[0] * 4 + off[1]
        return copy(part, part, (partner, tp), s_d.at[half, at], r_d.at[half, at])

    def arrived_across(half, off):
        rows = HALVES[half]
        at = off[0] * 4 + off[1]
        there = g.at[
            slot(*off), pl.ds(rows[0], rows[1]),
            pl.ds(pl.multiple_of((1 - core) * ROWS, 128), ROWS),
        ]
        return copy(there, there, (partner, tp), s_d.at[half, at], r_d.at[half, at])

    own_across = copy(
        block, g.at[slot(0, 0), :, lanes], (partner, tp), s_own.at[0], r_own.at[0]
    )

    barrier = pltpu.get_barrier_semaphore()
    for off in ((1, 0), (3, 0), (0, 1), (0, 3)):
        pl.semaphore_signal(barrier, inc=1, device_id=device(*off), device_id_type=MESH)
    pl.semaphore_signal(barrier, inc=1, device_id=(partner, tp), device_id_type=MESH)
    pl.semaphore_wait(barrier, 5)

    own_across.start()
    for half in range(2):
        for d in range(2):
            first_full(half, d).start()
    for half in range(2):
        for d in range(2):
            second_full(half, 0, d).start()

    acc[...] = jnp.zeros_like(acc)
    g[slot(0, 0), :, lanes] = block[...]
    wt[...] = w_up[...].astype(f32).T.astype(bf)
    for h in range(HEADS_HERE):
        kt[h, HEAD:128] = jnp.zeros((32, 2 * ROWS), bf)
        vt[h, VALUE_DIM:128] = jnp.where(
            lax.broadcasted_iota(jnp.int32, (64, 2 * ROWS), 0) == 0, 1.0, 0.0
        ).astype(bf)
    own_across.wait_recv()

    def neighbours():
        for half in range(2):
            for d in range(2):
                first_full(half, d).wait_recv()
                first_part(half, d).start()
        for half in range(2):
            for d in range(2):
                second_full(half, 0, d).wait_recv()
                second_part(half, 0, d).start()
        for half in range(2):
            for d in range(2):
                across_chip(half, offsets(half, STEPS[1 - d], 0)).start()
                across_chip(half, offsets(half, 0, STEPS[1 - d])).start()
        for half in range(2):
            for d in range(2):
                for e in range(2):
                    second_full(half, STEPS[1 - d], e).start()

    def opposite():
        for half in range(2):
            for d in range(2):
                first_part(half, d).wait_recv()
            for e in range(2):
                second_full(half, 2, e).start()
            across_chip(half, offsets(half, 2, 0)).start()
            for d in range(2):
                second_part(half, 0, d).wait_recv()
            across_chip(half, offsets(half, 0, 2)).start()

    def diagonal():
        for half in range(2):
            for along in STEPS:
                for d in range(2):
                    second_full(half, along, d).wait_recv()
                    second_part(half, along, d).start()
                    across_chip(half, offsets(half, along, STEPS[1 - d])).start()

    def far():
        for half in range(2):
            for d in range(2):
                second_full(half, 2, d).wait_recv()
                second_part(half, 2, d).start()
                across_chip(half, offsets(half, 2, STEPS[1 - d])).start()
            for along in STEPS:
                for d in range(2):
                    second_part(half, along, d).wait_recv()
                across_chip(half, offsets(half, along, 2)).start()

    def farthest():
        for half in range(2):
            for d in range(2):
                second_part(half, 2, d).wait_recv()
            across_chip(half, (2, 2)).start()

    def chosen(t, values):
        return sum(jnp.where(t == k, v, 0) for k, v in enumerate(values) if v)

    def step(t, carry):
        for at, event in zip(EVENTS, (neighbours, opposite, diagonal, far, farthest)):
            pl.when(t == at)(event)
        dy = chosen(t, [o[0] for o in ORDER])
        dz = chosen(t, [o[1] for o in ORDER])

        @pl.when(t > 0)
        def _():
            for half in range(2):
                arrived_across(half, (dy, dz)).wait_recv()

        at = slot(dy, dz)
        lat = g[at, 0:LATENT, :]
        rot = g[at, LATENT : LATENT + ROPE, :].astype(f32)
        squares = g[at, LATENT + ROPE : KEY_ROWS, :].astype(f32)
        squares = squares[0:1] + squares[1:2]
        for h in range(HEADS_HERE):
            kv = jnp.dot(wt[h * 128 : (h + 1) * 128, :], lat, preferred_element_type=f32)
            k = kv[0:NOPE]
            r = lax.rsqrt((jnp.sum(k * k, axis=0, keepdims=True) + squares) * (1.0 / HEAD) + eps)
            kt[h, 0:NOPE] = (k * r).astype(bf)
            kt[h, NOPE:HEAD] = (rot * r).astype(bf)
            vt[h, 0:VALUE_DIM] = kv[NOPE:128].astype(bf)
        for h in range(HEADS_HERE):
            scores = jnp.dot(q[h], kt[h], preferred_element_type=f32)
            weights = jnp.exp2(scores).astype(bf)
            acc[h] += lax.dot_general(
                weights, vt[h], (((1,), (1,)), ((), ())), preferred_element_type=f32
            )
        return carry

    lax.fori_loop(0, 16, step, 0)
    for h in range(HEADS_HERE):
        a = acc[h]
        out[:, h * VALUE_DIM : (h + 1) * VALUE_DIM] = (
            a[:, 0:VALUE_DIM] / a[:, VALUE_DIM : VALUE_DIM + 1]
        ).astype(bf)

    own_across.wait_send()
    for half in range(2):
        for d in range(2):
            first_full(half, d).wait_send()
            first_part(half, d).wait_send()
            for along in range(4):
                second_full(half, along, d).wait_send()
                second_part(half, along, d).wait_send()
        for off in ORDER[1:]:
            across_chip(half, off).wait_send()


def attend(q, block, w_up):
    vmem = pl.BlockSpec(memory_space=pltpu.VMEM)
    dma = pltpu.SemaphoreType.DMA
    sems = []
    for shape in ((1,), (2, 2), (2, 2), (2, 4, 2), (2, 4, 2), (2, 16)):
        sems += [dma(shape), dma(shape)]
    return pl.pallas_call(
        attend_kernel,
        out_shape=jax.ShapeDtypeStruct((ROWS, HEADS_HERE * VALUE_DIM), bf),
        in_specs=[vmem, vmem, vmem],
        out_specs=vmem,
        scratch_shapes=[
            pltpu.VMEM((16, KEY_ROWS, 2 * ROWS), bf),
            pltpu.VMEM((HEADS_HERE, ROWS, 128), f32),
            pltpu.VMEM((HEADS_HERE, 128, 2 * ROWS), bf),
            pltpu.VMEM((HEADS_HERE, 128, 2 * ROWS), bf),
            pltpu.VMEM((HEADS_HERE * 128, LATENT), bf),
        ]
        + sems,
        compiler_params=pltpu.CompilerParams(
            collective_id=1, has_side_effects=True, vmem_limit_bytes=40 * 2**20
        ),
        name="attend",
    )(q, block, w_up)


def extended(cells, width):
    count = lax.axis_size("sp")
    ends = count - 1
    head = cells[:width]
    tail = cells[-width:]
    return jnp.concatenate(
        [
            lax.ppermute(tail, "sp", [(i, (i + 1) % count) for i in range(ends)]),
            cells,
            lax.ppermute(head, "sp", [((i + 1) % count, i) for i in range(ends)]),
        ],
        axis=0,
    )


def gathered_copies(value, axis, dim):
    copies = jnp.broadcast_to(value, (lax.axis_size(axis), *value.shape))
    parts = lax.all_to_all(copies, axis, split_axis=0, concat_axis=0, tiled=True)
    lengths = list(value.shape)
    lengths[dim] *= parts.shape[0]
    return jnp.moveaxis(parts, 0, dim).reshape(lengths)


def body(
    tokens, norm_gain, w_query_down, query_gain, w_query_up, w_latent_down, latent_gain,
    w_rotary_key, w_latent_up, query_head_gain, key_head_gain, w_pool_in, w_pool_mix, pool_scale,
    w_attn_out, w_pool_out, w_gate_attn, w_gate_pool,
):
    rows = tokens.shape[0]
    length = rows * lax.axis_size("sp")
    positions = lax.axis_index("sp") * rows + jnp.arange(rows, dtype=jnp.int32)
    normed, block, query = front(
        tokens, norm_gain, w_query_down, query_gain, w_query_up, w_latent_down, latent_gain,
        w_rotary_key, query_head_gain, key_head_gain,
    )
    attn_rows = attend(query, block, w_latent_up)
    pool_input = jnp.dot(normed, w_pool_in, preferred_element_type=f32).astype(bf)
    reach = 8
    window = jnp.power(2, lax.axis_index("tp") + 1)
    padded = extended(pool_input, reach)
    offs = jnp.arange(rows + 2 * reach)[None, :] - reach - jnp.arange(rows)[:, None]
    band = ((offs >= -(window // 2)) & (offs < window // 2)).astype(bf)
    pooled = jnp.dot(band, padded, preferred_element_type=f32)
    low = jnp.clip(positions[:, None] - window // 2, 0, length)
    high = jnp.clip(positions[:, None] + window // 2, 0, length)
    count = (high - low).astype(f32)
    pool_mixed = (pooled / count - pool_input.astype(f32)).astype(bf)
    grouped = jnp.dot(pool_mixed, w_pool_mix[0], preferred_element_type=f32)
    pool_rows = (grouped * pool_scale).astype(bf)
    gate_attn = jax.nn.sigmoid(jnp.dot(normed, w_gate_attn, preferred_element_type=f32))
    gate_pool = jax.nn.sigmoid(jnp.dot(normed, w_gate_pool, preferred_element_type=f32))
    attn_tokens = lax.all_to_all(attn_rows, "tp", split_axis=0, concat_axis=1, tiled=True)
    pool_tokens = lax.all_to_all(pool_rows, "tp", split_axis=0, concat_axis=1, tiled=True)
    both = gathered_copies(jnp.concatenate([w_attn_out, w_pool_out], axis=1), "tp", 0)
    width = w_attn_out.shape[1]
    attn_here = jnp.dot(attn_tokens, both[:, :width], preferred_element_type=f32)
    pool_here = jnp.dot(pool_tokens, both[:, width:], preferred_element_type=f32)
    attn_branch = lax.all_to_all(attn_here.astype(bf), "tp", split_axis=1, concat_axis=0, tiled=True)
    pool_branch = lax.all_to_all(pool_here.astype(bf), "tp", split_axis=1, concat_axis=0, tiled=True)
    return (gate_attn * attn_branch.astype(f32) + gate_pool * pool_branch.astype(f32)).astype(bf)


def solution(mesh):
    placed = (
        P("sp", "tp"), P(), P(), P(), P(None, "tp"), P(), P(), P(), P(None, "tp"), P(), P(),
        P(None, "tp"), P("tp", None, None), P("tp"), P("tp", None), P("tp", None),
        P(None, "tp"), P(None, "tp"),
    )
    return jax.shard_map(body, mesh=mesh, in_specs=placed, out_specs=P("sp", "tp"), check_vma=False)
```

time: 306 us -> 238 us (0.78)
  matrix products: 87.7 us -> 17.8 us
  Pallas kernels: 0 us -> 64.2 us
  waiting for transfers between devices: 43.3 us -> 105 us
  local copies, waits for them, and re-layouts: 54.4 us -> 19.7 us
  other arithmetic: 31.3 us -> 2.97 us
  loops' own time: 25.1 us -> 0 us
  blocking collectives: 24.9 us -> 0 us
  between operations: 14.1 us -> 0.17 us
  starting transfers between devices: 22.9 us -> 26 us
    all_to_all x3, waiting for transfers between devices: 10.8 us -> 101 us  [the longest x1 93.1 us: gathered_copies(): lax.all_to_all(copies, axis, split_axis=0, concat_axis=0, tiled=True)]
    dot_general x106 -> x6, matrix products: 87.7 us -> 17.8 us  [the longest x1 4.1 us: body(): jnp.dot(normed, w_gate_pool, preferred_element_type=f32)]
    pallas_call x0 -> x2, Pallas kernels: none -> 64.2 us  [the longest x1 43.7 us: attend(): pl.pallas_call(attend_kernel, out_shape=jax.ShapeDtypeStruct((ROWS, HEADS...]
    another operation x1 -> x0, loops' own time: 25.1 us -> none  [body(): lax.scan(one_block, start_state, (latent_blocks, rotary_blocks, jnp.arang...]
    all_to_all x1 -> x0, blocking collectives: 24.9 us -> none  [sent_to_all(): return lax.all_to_all(copies, axis, split_axis=0, concat_axis=0, tiled=True)]
    all_gather x1 -> x0, waiting for transfers between devices: 22.1 us -> none  [side_by_side(): lax.all_gather(both, axis, axis=dim, tiled=True)]
    dynamic_slice x32 -> x0, local copies, waits for them, and re-layouts: 18.8 us -> none  [body(): lax.scan(one_block, start_state, (latent_blocks, rotary_blocks, jnp.arang...]
    reduce_sum x66 -> x0, other arithmetic: 13.7 us -> none  [the longest x32 10.7 us: one_block(): total = total * factor + jnp.sum(expo, axis=-1)]
  transfers between devices with their start and end apart: 8 -> 7, of which waited for: 6 -> 5; matrix products, arithmetic and copies ran while one was open for 54% -> 6% of each run, Pallas kernels for 0% -> 0%
where the time goes in v1:
time: 238 us; the launch traced here: 235 us
  waiting for transfers between devices  105 us (44%)
  Pallas kernels  64.2 us (27%)
  starting transfers between devices  26 us (11%)
  local copies, waits for them, and re-layouts  19.7 us (8%)
  matrix products  17.8 us (7%)
  other arithmetic  2.97 us (1%)
    all_to_all x1, waiting for transfers between devices, gathered_copies(): lax.all_to_all(copies, axis, split_axis=0, concat_axis=0, tiled=True)  93.1 us
    pallas_call x1, Pallas kernels, attend(): pl.pallas_call(attend_kernel, out_shape=jax.ShapeDtypeStruct((ROWS, HEADS...  43.7 us
    pallas_call x1, Pallas kernels, front(): pl.pallas_call(front_kernel, out_shape=(jax.ShapeDtypeStruct((ROWS, 2048)...  20.6 us
    unnamed x31, local copies, waits for them, and re-layouts  12.2 us
    broadcast_in_dim x1, local copies, waits for them, and re-layouts, gathered_copies(): copies = jnp.broadcast_to(value, (lax.axis_size(axis), *value.shape))  5.93 us
    all_to_all x1, starting transfers between devices, gathered_copies(): lax.all_to_all(copies, axis, split_axis=0, concat_axis=0, tiled=True)  5.69 us
    all_to_all x1, starting transfers between devices, body(): lax.all_to_all(pool_rows, 'tp', split_axis=0, concat_axis=1, tiled=True)  4.8 us
  transfers between devices with their start and end apart: 7, of which 5 were waited for; matrix products, arithmetic and copies ran while one was open for 6% of the time, Pallas kernels for 0%

profile of v1, /device:TPU:0, one launch (start us, length us, event | category | flops | bytes accessed | tf_op | source)
XLA Modules:
  0.0 235.5 jit_solution(13911939504944058292)
XLA Ops:
  0.0 0.0 copy-start
  0.0 1.3 copy.29.wr_h
  1.3 0.0 copy-start.1
  1.3 1.6 copy-done.1
  2.9 1.2 copy-done.2
  4.2 1.0 copy-done.3
  5.2 1.0 copy-done.4
  6.2 0.8 copy-done.6
  7.0 0.7 copy-done.7
  7.7 0.7 copy-done.8
  8.4 0.7 copy-done.9
  9.0 0.7 copy-done.10
  9.7 0.7 copy-done.11
  10.4 0.7 copy-done.12
  11.0 20.6 %front.1 = (bf16[384,2048]{1,0:T(8,128)(2,1)S(1)}, bf16[304,384]{1,0:T(8,128)(2,1)S(1)}, bf16[4,384,128]{2,1,0:T(8,128)(2,1)S(1)}) custom-call(bf16[384,512]{1,0:T(8,128)(2,1)S(1)} %copy-done.3, f32[1,2048]{1,0:T(1,128)S(1)} %bitcast.39, bf16[2048,512]{1,0:T(8,128)(2,1)S(1)} %copy-done.1, f32[1,512]{1,0:T(1,128)S(1)} %bitcast.40, ...), custom_call_target="tpu_custom_call" | custom-call | tf_op jit(solution)/shard_map/front/pallas_call | solution.py:183
  31.6 0.0 copy-start.13
  31.6 1.2 copy-done.13
  32.8 0.0 copy-done.5
  32.8 43.7 %attend.1 = bf16[384,256]{1,0:T(8,128)(2,1)} custom-call(bf16[4,384,128]{2,1,0:T(8,128)(2,1)S(1)} %get-tuple-element.9.q, bf16[304,384]{1,0:T(8,128)(2,1)S(1)} %get-tuple-element.10.block, bf16[256,512]{1,0:T(8,128)(2,1)S(1)} %copy-done.5), custom_call_target="tpu_custom_call" | custom-call | tf_op jit(solution)/shard_map/attend/pallas_call | solution.py:440
  76.5 3.6 %all-to-all-start = ((bf16[4,96,256]{2,1,0:T(8,128)(2,1)}), bf16[4,96,256]{2,1,0:T(8,128)(2,1)S(1)}, u32[]{:S(2)}, u32[]{:S(2)}) async-start(bf16[4,96,256]{2,1,0:T(8,128)(2,1)} %bitcast.5), calls=%async_computation | async-start | bytes 393216 | tf_op jit(solution)/shard_map/all_to_all | solution.py:511
  80.0 2.3 convolution_convert_fusion
  82.3 0.0 copy-start.14
  82.3 1.4 collective-permute-start.1
  83.8 3.6 %collective-permute-start = (bf16[8,256]{1,0:T(8,128)(2,1)S(1)}, bf16[8,256]{1,0:T(8,128)(2,1)}, u32[]{:S(2)}, u32[]{:S(2)}) collective-permute-start(bf16[8,256]{1,0:T(8,128)(2,1)S(1)} %get-tuple-element.11), channel_id=1, source_target_pairs={{0,4},{4,8},{8,12},{12,16},{16,20},{20,24},{24,28},{28,32},{32,36}... | collective-permute-start | bytes 12296 | tf_op jit(solution)/shard_map/ppermute | solution.py:467
  87.4 0.0 collective-permute-done.1
  87.4 0.3 collective-permute-done
  87.7 2.1 fusion.22
  89.8 0.0 all-to-all-done
  89.8 4.8 %all-to-all-start.3 = ((bf16[4,96,256]{2,1,0:T(8,128)(2,1)}), bf16[4,96,256]{2,1,0:T(8,128)(2,1)S(1)}, u32[]{:S(2)}, u32[]{:S(2)}) async-start(bf16[4,96,256]{2,1,0:T(8,128)(2,1)} %bitcast.50), calls=%async_computation.3 | async-start | bytes 393216 | tf_op jit(solution)/shard_map/all_to_all | solution.py:512
  94.6 0.0 copy-done.14
  94.6 2.8 %pad_maximum_fusion = bf16[256,4096]{1,0:T(8,128)(2,1)} fusion(bf16[256,2048]{1,0:T(8,128)(2,1)S(1)} %copy-done.14, bf16[256,2048]{1,0:T(8,128)(2,1)} %param.34), kind=kLoop, calls=%fused_computation.6 | loop fusion | flops 4194304 | bytes 4194304 | tf_op jit(solution)/shard_map/concatenate | solution.py:513
  97.4 3.7 %all-to-all-done.3 = bf16[4,96,256]{2,1,0:T(8,128)(2,1)S(1)} async-done(((bf16[4,96,256]{2,1,0:T(8,128)(2,1)}), bf16[4,96,256]{2,1,0:T(8,128)(2,1)S(1)}, u32[]{:S(2)}, u32[]{:S(2)}) %all-to-all-start.3) | async-done | bytes 196640 | tf_op jit(solution)/shard_map/all_to_all | solution.py:512
  101.1 5.9 %broadcast_in_dim.2 = bf16[4,256,4096]{2,1,0:T(8,128)(2,1)} broadcast(bf16[256,4096]{1,0:T(8,128)(2,1)} %pad_maximum_fusion), dimensions={1,2} | broadcast | bytes 10485760 | tf_op jit(solution)/shard_map/broadcast_in_dim | solution.py:476
  107.0 5.7 %all-to-all-start.1 = ((bf16[4,256,4096]{2,1,0:T(8,128)(2,1)}), bf16[4,256,4096]{2,1,0:T(8,128)(2,1)}, u32[]{:S(2)}, u32[]{:S(2)}) async-start(bf16[4,256,4096]{2,1,0:T(8,128)(2,1)} %broadcast_in_dim.2), calls=%async_computation.1 | async-start | bytes 16777216 | tf_op jit(solution)/shard_map/all_to_all | solution.py:477
  112.8 93.1 %all-to-all-done.1 = bf16[4,256,4096]{2,1,0:T(8,128)(2,1)} async-done(((bf16[4,256,4096]{2,1,0:T(8,128)(2,1)}), bf16[4,256,4096]{2,1,0:T(8,128)(2,1)}, u32[]{:S(2)}, u32[]{:S(2)}) %all-to-all-start.1) | async-done | bytes 8388640 | tf_op jit(solution)/shard_map/all_to_all | solution.py:477
  205.9 3.0 %fusion.4 = bf16[96,2048]{1,0:T(8,128)(2,1)S(1)} fusion(bf16[96,1024]{1,0:T(8,128)(2,1)S(1)} %bitcast.52, bf16[1024,4096]{1,0:T(8,128)(2,1)} %bitcast.7), kind=kOutput, calls=%fused_computation.4 | convolution fusion | flops 402849792 | bytes 4784128 | tf_op jit(solution)/shard_map/dot_general | solution.py:515
  208.9 0.8 copy.41
  209.7 3.5 %all-to-all-start.2 = ((bf16[96,4,512]{2,0,1:T(8,128)(2,1)}), bf16[96,4,512]{2,0,1:T(8,128)(2,1)S(1)}, u32[]{:S(2)}, u32[]{:S(2)}) async-start(bf16[96,4,512]{2,0,1:T(8,128)(2,1)} %bitcast.38), calls=%async_computation.2 | async-start | bytes 786432 | tf_op jit(solution)/shard_map/all_to_all | solution.py:517
  213.1 3.0 %fusion.7 = bf16[96,2048]{1,0:T(8,128)(2,1)S(1)} fusion(bf16[96,1024]{1,0:T(8,128)(2,1)S(1)} %bitcast.51, bf16[1024,4096]{1,0:T(8,128)(2,1)} %bitcast.7), kind=kOutput, calls=%fused_computation.5 | convolution fusion | flops 402849792 | bytes 4784128 | tf_op jit(solution)/shard_map/dot_general | solution.py:516
  216.1 0.8 copy.40
  216.9 3.6 %all-to-all-done.2 = bf16[96,4,512]{2,0,1:T(8,128)(2,1)S(1)} async-done(((bf16[96,4,512]{2,0,1:T(8,128)(2,1)}), bf16[96,4,512]{2,0,1:T(8,128)(2,1)S(1)}, u32[]{:S(2)}, u32[]{:S(2)}) %all-to-all-start.2) | async-done | bytes 393248 | tf_op jit(solution)/shard_map/all_to_all | solution.py:517
  220.5 3.5 %all-to-all-start.4 = ((bf16[96,4,512]{2,0,1:T(8,128)(2,1)}), bf16[96,4,512]{2,0,1:T(8,128)(2,1)S(1)}, u32[]{:S(2)}, u32[]{:S(2)}) async-start(bf16[96,4,512]{2,0,1:T(8,128)(2,1)} %bitcast.37), calls=%async_computation.4 | async-start | bytes 786432 | tf_op jit(solution)/shard_map/all_to_all | solution.py:518
  224.0 0.1 convert_element_type.64
  224.0 0.0 copy-done
  224.1 3.4 %fusion.14 = f32[384,512]{1,0:T(8,128)} fusion(f32[384,512]{1,0:T(8,128)S(1)} %bitcast.45, bf16[384,2048]{1,0:T(8,128)(2,1)} %copy-done.13, bf16[2048,512]{1,0:T(8,128)(2,1)S(1)} %copy-done), kind=kOutput, calls=%fused_computation.13 | convolution fusion | flops 806092800 | bytes 5242880 | tf_op jit(solution)/shard_map/dot_general | solution.py:509
  227.4 3.9 %all-to-all-done.4 = bf16[96,4,512]{2,0,1:T(8,128)(2,1)S(1)} async-done(((bf16[96,4,512]{2,0,1:T(8,128)(2,1)}), bf16[96,4,512]{2,0,1:T(8,128)(2,1)S(1)}, u32[]{:S(2)}, u32[]{:S(2)}) %all-to-all-start.4) | async-done | bytes 393248 | tf_op jit(solution)/shard_map/all_to_all | solution.py:518
  231.3 0.1 convert_element_type.65
  231.4 4.1 %fusion.19 = bf16[384,512]{1,0:T(8,128)(2,1)} fusion(f32[384,512]{1,0:T(8,128)} %fusion.14, f32[384,512]{1,0:T(8,128)S(1)} %bitcast.44, bf16[384,2048]{1,0:T(8,128)(2,1)} %copy-done.13, bf16[2048,512]{1,0:T(8,128)(2,1)} %param.37), kind=kOutput, calls=%fused_computation.18 | convolution fusion | flops 806486016 | bytes 5636096 | tf_op jit(solution)/shard_map/dot_general | solution.py:510
  (16 shorter events, 0.1 us)
Async XLA Ops:
  0.0 224.0 %copy-start = (bf16[2048,512]{1,0:T(8,128)(2,1)S(1)}, bf16[2048,512]{1,0:T(8,128)(2,1)}, u32[]{:S(2)}) copy-start(bf16[2048,512]{1,0:T(8,128)(2,1)} %param.36) | copy-start | bytes 6291460
  1.3 1.6 copy-start.1
  2.9 1.2 copy-start.2
  4.2 1.0 copy-start.3
  5.2 1.0 copy-start.4
  6.1 0.8 copy-start.6
  6.9 0.7 copy-start.7
  7.7 0.7 copy-start.8
  8.4 0.7 copy-start.9
  9.0 0.7 copy-start.10
  9.7 0.7 copy-start.11
  10.4 0.7 copy-start.12
  11.0 21.7 %copy-start.5 = (bf16[256,512]{1,0:T(8,128)(2,1)S(1)}, bf16[256,512]{1,0:T(8,128)(2,1)}, u32[]{:S(2)}) copy-start(bf16[256,512]{1,0:T(8,128)(2,1)} %w_up.1) | copy-start | bytes 786436
  31.6 1.2 copy-start.13
  76.5 13.4 %all-to-all-start = ((bf16[4,96,256]{2,1,0:T(8,128)(2,1)}), bf16[4,96,256]{2,1,0:T(8,128)(2,1)S(1)}, u32[]{:S(2)}, u32[]{:S(2)}) async-start(bf16[4,96,256]{2,1,0:T(8,128)(2,1)} %bitcast.5), calls=%async_computation | async-start | bytes 393216 | tf_op jit(solution)/shard_map/all_to_all | solution.py:511
  82.3 12.3 %copy-start.14 = (bf16[256,2048]{1,0:T(8,128)(2,1)S(1)}, bf16[256,2048]{1,0:T(8,128)(2,1)}, u32[]{:S(2)}) copy-start(bf16[256,2048]{1,0:T(8,128)(2,1)} %param.35) | copy-start | bytes 3145732
  82.3 5.1 %collective-permute-start.1 = (bf16[8,256]{1,0:T(8,128)(2,1)S(1)}, bf16[8,256]{1,0:T(8,128)(2,1)}, u32[]{:S(2)}, u32[]{:S(2)}) collective-permute-start(bf16[8,256]{1,0:T(8,128)(2,1)S(1)} %get-tuple-element.12), channel_id=1, source_target_pairs={{4,0},{8,4},{12,8},{16,12},{20,16},{24,20},{28,24},{32,28},{36,32}... | collective-permute-start | bytes 12296 | tf_op jit(solution)/shard_map/ppermute | solution.py:469
  83.8 4.0 %collective-permute-start = (bf16[8,256]{1,0:T(8,128)(2,1)S(1)}, bf16[8,256]{1,0:T(8,128)(2,1)}, u32[]{:S(2)}, u32[]{:S(2)}) collective-permute-start(bf16[8,256]{1,0:T(8,128)(2,1)S(1)} %get-tuple-element.11), channel_id=1, source_target_pairs={{0,4},{4,8},{8,12},{12,16},{16,20},{20,24},{24,28},{28,32},{32,36}... | collective-permute-start | bytes 12296 | tf_op jit(solution)/shard_map/ppermute | solution.py:467
  89.8 11.3 %all-to-all-start.3 = ((bf16[4,96,256]{2,1,0:T(8,128)(2,1)}), bf16[4,96,256]{2,1,0:T(8,128)(2,1)S(1)}, u32[]{:S(2)}, u32[]{:S(2)}) async-start(bf16[4,96,256]{2,1,0:T(8,128)(2,1)} %bitcast.50), calls=%async_computation.3 | async-start | bytes 393216 | tf_op jit(solution)/shard_map/all_to_all | solution.py:512
  107.0 98.9 %all-to-all-start.1 = ((bf16[4,256,4096]{2,1,0:T(8,128)(2,1)}), bf16[4,256,4096]{2,1,0:T(8,128)(2,1)}, u32[]{:S(2)}, u32[]{:S(2)}) async-start(bf16[4,256,4096]{2,1,0:T(8,128)(2,1)} %broadcast_in_dim.2), calls=%async_computation.1 | async-start | bytes 16777216 | tf_op jit(solution)/shard_map/all_to_all | solution.py:477
  209.7 10.8 %all-to-all-start.2 = ((bf16[96,4,512]{2,0,1:T(8,128)(2,1)}), bf16[96,4,512]{2,0,1:T(8,128)(2,1)S(1)}, u32[]{:S(2)}, u32[]{:S(2)}) async-start(bf16[96,4,512]{2,0,1:T(8,128)(2,1)} %bitcast.38), calls=%async_computation.2 | async-start | bytes 786432 | tf_op jit(solution)/shard_map/all_to_all | solution.py:517
  220.5 10.8 %all-to-all-start.4 = ((bf16[96,4,512]{2,0,1:T(8,128)(2,1)}), bf16[96,4,512]{2,0,1:T(8,128)(2,1)S(1)}, u32[]{:S(2)}, u32[]{:S(2)}) async-start(bf16[96,4,512]{2,0,1:T(8,128)(2,1)} %bitcast.37), calls=%async_computation.4 | async-start | bytes 786432 | tf_op jit(solution)/shard_map/all_to_all | solution.py:518

commit v2 on v1

v2 whole, which is shorter than its diff:
```python
import numpy as np
import jax
import jax.numpy as jnp
from jax import lax
from jax.experimental import pallas as pl
from jax.experimental.pallas import tpu as pltpu
from jax.sharding import PartitionSpec as P

NOPE = 64
ROPE = 32
HEAD = NOPE + ROPE
VALUE_DIM = 64
ROWS = 384
HEADS_HERE = 4
LATENT = 256
KEY_ROWS = 304
CHUNK = 128
CHUNKS = 3
MESH = pl.DeviceIdType.MESH

eps = 1e-06
theta = 10000.0
LOG2E = 1.4426950408889634
bf = jnp.bfloat16
f32 = jnp.float32


def rope_tables():
    half = ROPE // 2
    freqs = theta ** (-np.arange(half, dtype=np.float64) / half)
    fine = np.arange(ROWS)[None, :] * freqs[:, None]
    coarse = (np.arange(128) * ROWS)[None, :] * freqs[:, None]
    fine = np.stack([np.cos(fine), np.sin(fine)]).astype(np.float32)
    coarse = np.stack([np.cos(coarse), np.sin(coarse)]).astype(np.float32)
    return fine, coarse


def column(row):
    wide = jnp.concatenate([row, jnp.zeros((1, 128 - row.shape[1]), f32)], axis=1)
    return jnp.broadcast_to(wide, (128, 128)).T


ORDER = (
    (0, 0),
    (3, 0), (1, 0), (0, 3), (0, 1),
    (2, 0), (0, 2),
    (3, 3), (3, 1), (1, 3), (1, 1),
    (3, 2), (1, 2), (2, 3), (2, 1),
    (2, 2),
)
HALVES = ((0, 160), (160, 144))
PARTS = (((0, 80), (80, 80)), ((160, 80), (240, 64)))
STEPS = (1, 3)


def mixer_kernel(
    tok, ng_h, wq_h, qg_h, wu_h, wl_h, lg_h, wr_h, wup_h, qhg_h, khg_h, wpi_h, mix_h, ps_h,
    wao_h, wpo_h, wga_h, wgp_h, fine_h, coarse_h,
    out,
    whole, ng, wq, qg, wu, wl, lg, wr, w_up, qhg, khg, wpi, mix, ps, wg, fine, coarse,
    normed, block, q, padded, g, acc, kt, vt, wt, gates, w_out, stage, prow, arow,
    load_sem, tok_sem, wown_sem, xt, xa, xp, xw, halo, s_across, r_across,
    s_1f, r_1f, s_1h, r_1h, s_2o, r_2o, s_2f, r_2f, s_2h, r_2h, s_d, r_d,
):
    sp = lax.axis_index("sp")
    tp = lax.axis_index("tp")
    core, y, z = sp % 2, (sp // 2) % 4, sp // 8
    partner = sp + 1 - 2 * core
    right, left, opposite_x = (tp + 1) % 4, (tp + 3) % 4, (tp + 2) % 4

    def copy(src, dst, to, send, recv):
        return pltpu.make_async_remote_copy(
            src_ref=src, dst_ref=dst, send_sem=send, recv_sem=recv,
            device_id=to, device_id_type=MESH,
        )

    def slot(dy, dz):
        return ((z + dz) % 4) * 4 + (y + dy) % 4

    def device(dy, dz):
        return (slot(dy, dz) * 2 + core, tp)

    def offsets(half, along, across):
        return (along, across) if half == 0 else (across, along)

    def lanes(c=None, whose=core):
        if c is None:
            return pl.ds(pl.multiple_of(whose * ROWS, 128), ROWS)
        return pl.ds(pl.multiple_of(whose * ROWS + c * CHUNK, 128), CHUNK)

    def chunk(c):
        return pl.ds(pl.multiple_of(c * CHUNK, 128), CHUNK)

    def region(off, rows, c=None):
        return g.at[slot(*off), pl.ds(rows[0], rows[1]), lanes(c)]

    def own_first(half, d, c):
        rows = HALVES[half]
        return copy(
            block.at[pl.ds(rows[0], rows[1]), chunk(c)], region((0, 0), rows, c),
            device(*offsets(half, STEPS[d], 0)), s_1f.at[half, d, c], r_1f.at[half, d, c],
        )

    def own_second(half, d, c):
        rows = HALVES[half]
        return copy(
            block.at[pl.ds(rows[0], rows[1]), chunk(c)], region((0, 0), rows, c),
            device(*offsets(half, 0, STEPS[d])), s_2o.at[half, d, c], r_2o.at[half, d, c],
        )

    def own_across(c):
        return copy(
            block.at[:, chunk(c)], g.at[slot(0, 0), :, lanes(c)], (partner, tp),
            s_across.at[c], r_across.at[c],
        )

    def first_part(half, d):
        part = region(offsets(half, STEPS[1 - d], 0), PARTS[half][d])
        return copy(
            part, part, device(*offsets(half, STEPS[d], 0)),
            s_1h.at[half, d], r_1h.at[half, d],
        )

    def second_full(half, along, d):
        part = region(offsets(half, along, 0), HALVES[half])
        return copy(
            part, part, device(*offsets(half, 0, STEPS[d])),
            s_2f.at[half, along, d], r_2f.at[half, along, d],
        )

    def second_part(half, along, d):
        part = region(offsets(half, along, STEPS[1 - d]), PARTS[half][d])
        return copy(
            part, part, device(*offsets(half, 0, STEPS[d])),
            s_2h.at[half, along, d], r_2h.at[half, along, d],
        )

    def across_chip(half, off):
        part = region(off, HALVES[half])
        at = off[0] * 4 + off[1]
        return copy(part, part, (partner, tp), s_d.at[half, at], r_d.at[half, at])

    def arrived_across(half, off):
        rows = HALVES[half]
        at = off[0] * 4 + off[1]
        there = g.at[slot(*off), pl.ds(rows[0], rows[1]), lanes(whose=1 - core)]
        return copy(there, there, (partner, tp), s_d.at[half, at], r_d.at[half, at])

    def along_x(buf, first, n, sem, kind, i):
        to = right if kind % 2 == 0 else left
        if kind < 2:
            part = buf.at[tp, pl.ds(first, n)]
        elif kind == 2:
            part = buf.at[left, pl.ds(first, n // 2)]
        else:
            part = buf.at[right, pl.ds(pl.multiple_of(first + n // 2, 16), n // 2)]
        return copy(part, part, (sp, to), sem.at[0, kind, i], sem.at[1, kind, i])

    def token_copy(kind, c):
        return along_x(whole, pl.multiple_of(c * CHUNK, CHUNK), CHUNK, xt, kind, c)

    def attn_copy(kind, c):
        return along_x(arow, c * CHUNK, CHUNK, xa, kind, c)

    def pool_copy(kind):
        return along_x(prow, 0, ROWS, xp, kind, 0)

    def columns(j):
        return pl.ds(pl.multiple_of(j * 512, 512), 512)

    w_src = (wao_h, wpo_h)

    def weight_copy(kind, w):
        to = right if kind % 2 == 0 else left
        if kind < 2:
            src, dst = w_src[w].at[:, columns(to)], w_out.at[w, tp]
        elif kind < 4:
            src = w_src[w].at[pl.ds(128 * (kind - 2), 128), columns(opposite_x)]
            dst = stage.at[w, kind - 2]
        else:
            src = stage.at[w, kind - 4]
            dst = w_out.at[w, left if kind == 4 else right, pl.ds(128 * (kind - 4), 128)]
        return copy(src, dst, (sp, to), xw.at[0, kind, w], xw.at[1, kind, w])

    def halo_copy(kind):
        if kind == 0:
            src, dst, to = padded.at[384:400], padded.at[0:16], (sp + 1) % 32
        else:
            src, dst, to = padded.at[16:32], padded.at[400:416], (sp + 31) % 32
        return copy(src, dst, (to, tp), halo.at[0, kind], halo.at[1, kind])

    own_tokens = pltpu.make_async_copy(tok, whole.at[tp], tok_sem.at[0])
    own_tokens.start()
    pairs = (
        (ng_h, ng), (fine_h, fine), (coarse_h, coarse), (qhg_h, qhg), (khg_h, khg), (lg_h, lg),
        (qg_h, qg), (wl_h, wl), (wr_h, wr), (wq_h, wq), (wu_h, wu), (wpi_h, wpi),
        (mix_h, mix), (ps_h, ps), (wup_h, w_up), (wga_h, wg.at[0]), (wgp_h, wg.at[1]),
    )
    loads = [pltpu.make_async_copy(s, d, load_sem.at[i]) for i, (s, d) in enumerate(pairs)]
    for load in loads:
        load.start()
    own_weights = [
        pltpu.make_async_copy(w_src[w].at[:, columns(tp)], w_out.at[w, tp], wown_sem.at[w])
        for w in range(2)
    ]

    barrier = pltpu.get_barrier_semaphore()
    far_neighbour = jnp.where(core == 0, (sp + 31) % 32, (sp + 1) % 32)
    peers = [(sp, right), (sp, left), (partner, tp), (far_neighbour, tp)]
    peers += [device(*off) for off in ((1, 0), (3, 0), (0, 1), (0, 3))]
    for peer in peers:
        pl.semaphore_signal(barrier, inc=1, device_id=peer, device_id_type=MESH)
    own_tokens.wait()
    pl.semaphore_wait(barrier, len(peers))

    for c in range(2):
        for kind in range(2):
            token_copy(kind, c).start()
    for load in loads[:7]:
        load.wait()
    pick = lax.broadcasted_iota(jnp.int32, (16, 128), 1) == sp
    cc = jnp.sum(jnp.where(pick, coarse[0], 0.0), axis=1, keepdims=True)
    cs = jnp.sum(jnp.where(pick, coarse[1], 0.0), axis=1, keepdims=True)
    q_gain = column(qhg[...])
    k_gain = column(khg[...])
    for kind in range(2):
        token_copy(kind, 0).wait_recv()
        token_copy(kind + 2, 0).start()
    for kind in range(2):
        token_copy(kind, 2).start()
    for load in loads[7:]:
        load.wait()

    def front_step(c, carry):
        @pl.when(c < CHUNKS - 1)
        def _():
            for kind in range(2):
                token_copy(kind, c + 1).wait_recv()
                token_copy(kind + 2, c + 1).start()

        for kind in range(2):
            token_copy(kind + 2, c).wait_recv()
        rows = chunk(c)
        squares = jnp.zeros((CHUNK, 1), f32)
        for k in range(4):
            v = whole[k, rows].astype(f32)
            squares = squares + jnp.sum(v * v, axis=1, keepdims=True)
        scale = lax.rsqrt(squares * (1.0 / 2048) + eps)
        for k in range(4):
            v = whole[k, rows].astype(f32)
            normed[rows, k * 512 : (k + 1) * 512] = (
                v * scale * ng[:, k * 512 : (k + 1) * 512]
            ).astype(bf)
        here = normed[rows, :]
        lat = jnp.dot(here, wl[...], preferred_element_type=f32).astype(bf).astype(f32)
        lat = lat * lax.rsqrt(jnp.mean(lat * lat, axis=1, keepdims=True) + eps) * lg[...]
        lat = lat.T.astype(bf)
        fc, fs = fine[0, :, rows], fine[1, :, rows]
        cosine = cc * fc - cs * fs
        sine = cs * fc + cc * fs

        def rotated(first, second):
            return first * cosine - second * sine, first * sine + second * cosine

        rot = lax.dot_general(
            wr[...], here, (((1,), (1,)), ((), ())), preferred_element_type=f32
        ).astype(bf).astype(f32)
        total = jnp.sum(rot * rot, axis=0, keepdims=True)
        high = total.astype(bf).astype(f32)
        low = total - high
        rot = rot * k_gain[NOPE:HEAD]
        first, second = rotated(rot[0:16], rot[16:32])
        line = lax.broadcasted_iota(jnp.int32, (16, CHUNK), 0)
        tail = jnp.where(line == 0, high, jnp.where(line == 1, low, 0.0))
        made = jnp.concatenate(
            [lat, first.astype(bf), second.astype(bf), tail.astype(bf)], axis=0
        )
        block[:, rows] = made
        g[slot(0, 0), :, lanes(c)] = made

        lat = jnp.dot(here, wq[...], preferred_element_type=f32).astype(bf).astype(f32)
        lat = lat * lax.rsqrt(jnp.mean(lat * lat, axis=1, keepdims=True) + eps) * qg[...]
        raw = jnp.dot(lat.astype(bf), wu[...], preferred_element_type=f32)
        own_across(c).start()
        for half in range(2):
            for d in range(2):
                own_first(half, d, c).start()
        for half in range(2):
            for d in range(2):
                own_second(half, d, c).start()
        raw = raw.astype(bf).astype(f32).T
        for h in range(HEADS_HERE):
            v = raw[h * HEAD : (h + 1) * HEAD]
            r = lax.rsqrt(jnp.mean(v * v, axis=0, keepdims=True) + eps)
            v = v * (r * (HEAD ** (-0.5) * LOG2E)) * q_gain[0:HEAD]
            first, second = rotated(v[64:80], v[80:96])
            v = jnp.concatenate(
                [v[0:NOPE] * k_gain[0:NOPE], first, second, jnp.zeros((32, CHUNK), f32)], axis=0
            )
            q[h, rows, :] = v.T.astype(bf)
        padded[pl.ds(pl.multiple_of(c * CHUNK + 16, 16), CHUNK), :] = jnp.dot(
            here, wpi[...], preferred_element_type=f32
        ).astype(bf)
        return carry

    lax.fori_loop(0, CHUNKS, front_step, 0)
    for w in range(2):
        for kind in (2, 3):
            weight_copy(kind, w).start()
    for kind in (0, 1):
        weight_copy(kind, 0).start()
    for own in own_weights:
        own.start()

    acc[...] = jnp.zeros_like(acc)
    wt[...] = w_up[...].astype(f32).T.astype(bf)
    for h in range(HEADS_HERE):
        kt[h, HEAD:128] = jnp.zeros((32, 2 * ROWS), bf)
        vt[h, VALUE_DIM:128] = jnp.where(
            lax.broadcasted_iota(jnp.int32, (64, 2 * ROWS), 0) == 0, 1.0, 0.0
        ).astype(bf)
    for kind in range(2):
        halo_copy(kind).start()
    for c in range(CHUNKS):
        own_across(c).wait_recv()

    def gates_and_pool():
        for k in range(2):
            for n in range(2):
                cols = slice(n * 256, (n + 1) * 256)
                gates[k, :, cols] = jax.nn.sigmoid(
                    jnp.dot(normed[...], wg[k, :, cols], preferred_element_type=f32)
                )
        for kind in range(2):
            halo_copy(kind).wait_recv()
        reach = jnp.where(tp == 0, 1, jnp.where(tp == 1, 2, jnp.where(tp == 2, 4, 8)))
        source = lax.broadcasted_iota(jnp.int32, (ROWS, ROWS + 32), 1) - 16
        offs = source - lax.broadcasted_iota(jnp.int32, (ROWS, ROWS + 32), 0)
        source = source + sp * ROWS
        length = 32 * ROWS
        inside = (offs >= -reach) & (offs < reach) & (source >= 0) & (source < length)
        band = jnp.where(inside, 1.0, 0.0).astype(bf)
        pooled = jnp.dot(band, padded[...], preferred_element_type=f32)
        at = sp * ROWS + lax.broadcasted_iota(jnp.int32, (ROWS, 1), 0)
        count = (jnp.minimum(at + reach, length) - jnp.maximum(at - reach, 0)).astype(f32)
        mixed = (pooled / count - padded[16:400].astype(f32)).astype(bf)
        grouped = jnp.dot(mixed, mix[0], preferred_element_type=f32)
        prow[tp] = (grouped * ps[...]).astype(bf)

    def neighbours():
        for half in range(2):
            for d in range(2):
                for c in range(CHUNKS):
                    own_first(half, d, c).wait_recv()
                first_part(half, d).start()
        for half in range(2):
            for d in range(2):
                for c in range(CHUNKS):
                    own_second(half, d, c).wait_recv()
                second_part(half, 0, d).start()
        for half in range(2):
            for d in range(2):
                across_chip(half, offsets(half, STEPS[1 - d], 0)).start()
                across_chip(half, offsets(half, 0, STEPS[1 - d])).start()
        for half in range(2):
            for d in range(2):
                for e in range(2):
                    second_full(half, STEPS[1 - d], e).start()

    def send_pool():
        for kind in range(2):
            pool_copy(kind).start()

    def opposite():
        for half in range(2):
            for d in range(2):
                first_part(half, d).wait_recv()
            for e in range(2):
                second_full(half, 2, e).start()
            across_chip(half, offsets(half, 2, 0)).start()
            for d in range(2):
                second_part(half, 0, d).wait_recv()
            across_chip(half, offsets(half, 0, 2)).start()

    def pass_weights():
        for w in range(2):
            for kind in (2, 3):
                weight_copy(kind, w).wait_recv()
                weight_copy(kind + 2, w).start()
        for kind in (0, 1):
            weight_copy(kind, 1).start()

    def diagonal():
        for half in range(2):
            for along in STEPS:
                for d in range(2):
                    second_full(half, along, d).wait_recv()
                    second_part(half, along, d).start()
                    across_chip(half, offsets(half, along, STEPS[1 - d])).start()

    def pass_pool():
        for kind in range(2):
            pool_copy(kind).wait_recv()
            pool_copy(kind + 2).start()

    def far():
        for half in range(2):
            for d in range(2):
                second_full(half, 2, d).wait_recv()
                second_part(half, 2, d).start()
                across_chip(half, offsets(half, 2, STEPS[1 - d])).start()
            for along in STEPS:
                for d in range(2):
                    second_part(half, along, d).wait_recv()
                across_chip(half, offsets(half, along, 2)).start()

    def farthest():
        for half in range(2):
            for d in range(2):
                second_part(half, 2, d).wait_recv()
            across_chip(half, (2, 2)).start()

    events = (
        (1, gates_and_pool), (1, neighbours), (1, send_pool), (3, opposite), (4, pass_weights),
        (6, diagonal), (8, pass_pool), (9, far), (11, farthest),
    )

    def chosen(t, values):
        return sum(jnp.where(t == k, v, 0) for k, v in enumerate(values) if v)

    def step(t, carry):
        for at, event in events:
            pl.when(t == at)(event)
        dy = chosen(t, [o[0] for o in ORDER])
        dz = chosen(t, [o[1] for o in ORDER])

        @pl.when(t > 0)
        def _():
            for half in range(2):
                arrived_across(half, (dy, dz)).wait_recv()

        at = slot(dy, dz)
        lat = g[at, 0:LATENT, :]
        rot = g[at, LATENT : LATENT + ROPE, :].astype(f32)
        squares = g[at, LATENT + ROPE : KEY_ROWS, :].astype(f32)
        squares = squares[0:1] + squares[1:2]
        for h in range(HEADS_HERE):
            kv = jnp.dot(wt[h * 128 : (h + 1) * 128, :], lat, preferred_element_type=f32)
            k = kv[0:NOPE]
            r = lax.rsqrt((jnp.sum(k * k, axis=0, keepdims=True) + squares) * (1.0 / HEAD) + eps)
            kt[h, 0:NOPE] = (k * r).astype(bf)
            kt[h, NOPE:HEAD] = (rot * r).astype(bf)
            vt[h, 0:VALUE_DIM] = kv[NOPE:128].astype(bf)
        for h in range(HEADS_HERE):
            scores = jnp.dot(q[h], kt[h], preferred_element_type=f32)
            weights = jnp.exp2(scores).astype(bf)
            acc[h] += lax.dot_general(
                weights, vt[h], (((1,), (1,)), ((), ())), preferred_element_type=f32
            )
        return carry

    lax.fori_loop(0, 16, step, 0)

    for c in range(CHUNKS):
        rows = slice(c * CHUNK, (c + 1) * CHUNK)
        for h in range(HEADS_HERE):
            a = acc[h, rows]
            arow[tp, rows, h * VALUE_DIM : (h + 1) * VALUE_DIM] = (
                a[:, 0:VALUE_DIM] / a[:, VALUE_DIM : VALUE_DIM + 1]
            ).astype(bf)
        if c > 0:
            for kind in range(2):
                attn_copy(kind, c - 1).start()
    for own in own_weights:
        own.wait()
    for w in range(2):
        for kind in (0, 1, 4, 5):
            weight_copy(kind, w).wait_recv()
    for kind in range(2):
        attn_copy(kind, CHUNKS - 1).start()
        pool_copy(kind + 2).wait_recv()

    def projected(buf, rows, w):
        return sum(
            jnp.dot(buf[k, rows], w_out[w, k], preferred_element_type=f32) for k in range(4)
        )

    everything = slice(0, ROWS)
    gates[1] = gates[1] * projected(prow, everything, 1)
    for c in range(CHUNKS):
        for kind in range(2):
            attn_copy(kind, c).wait_recv()
            attn_copy(kind + 2, c).start()
    for c in range(CHUNKS):
        rows = slice(c * CHUNK, (c + 1) * CHUNK)
        for kind in range(2):
            attn_copy(kind + 2, c).wait_recv()
        out[rows, :] = (gates[0, rows] * projected(arow, rows, 0) + gates[1, rows]).astype(bf)

    for c in range(CHUNKS):
        for kind in range(4):
            token_copy(kind, c).wait_send()
            attn_copy(kind, c).wait_send()
        own_across(c).wait_send()
        for half in range(2):
            for d in range(2):
                own_first(half, d, c).wait_send()
                own_second(half, d, c).wait_send()
    for kind in range(4):
        pool_copy(kind).wait_send()
    for w in range(2):
        for kind in range(6):
            weight_copy(kind, w).wait_send()
    for half in range(2):
        halo_copy(half).wait_send()
        for d in range(2):
            first_part(half, d).wait_send()
            for along in range(4):
                if along:
                    second_full(half, along, d).wait_send()
                second_part(half, along, d).wait_send()
        for off in ORDER[1:]:
            across_chip(half, off).wait_send()


def body(
    tokens, norm_gain, w_query_down, query_gain, w_query_up, w_latent_down, latent_gain,
    w_rotary_key, w_latent_up, query_head_gain, key_head_gain, w_pool_in, w_pool_mix, pool_scale,
    w_attn_out, w_pool_out, w_gate_attn, w_gate_pool,
):
    fine, coarse = rope_tables()

    def row(v):
        return v.reshape(1, -1)

    args = (
        tokens, row(norm_gain), w_query_down, row(query_gain), w_query_up, w_latent_down,
        row(latent_gain), w_rotary_key.T, w_latent_up, row(query_head_gain), row(key_head_gain),
        w_pool_in, w_pool_mix, row(pool_scale), w_attn_out, w_pool_out, w_gate_attn, w_gate_pool,
        fine, coarse,
    )
    dma = pltpu.SemaphoreType.DMA
    sems = [dma((17,)), dma((1,)), dma((2,)), dma((2, 4, 3)), dma((2, 4, 3)), dma((2, 4, 1))]
    sems += [dma((2, 6, 2)), dma((2, 2)), dma((3,)), dma((3,))]
    for shape in ((2, 2, 3), (2, 2), (2, 2, 3), (2, 4, 2), (2, 4, 2), (2, 16)):
        sems += [dma(shape), dma(shape)]
    return pl.pallas_call(
        mixer_kernel,
        out_shape=jax.ShapeDtypeStruct((ROWS, 512), bf),
        in_specs=[pl.BlockSpec(memory_space=pl.ANY)] * len(args),
        out_specs=pl.BlockSpec(memory_space=pltpu.VMEM),
        scratch_shapes=[
            pltpu.VMEM((4, ROWS, 512), bf),
            pltpu.VMEM((1, 2048), f32),
            pltpu.VMEM((2048, 512), bf),
            pltpu.VMEM((1, 512), f32),
            pltpu.VMEM((512, 384), bf),
            pltpu.VMEM((2048, 256), bf),
            pltpu.VMEM((1, 256), f32),
            pltpu.VMEM((32, 2048), bf),
            pltpu.VMEM((256, 512), bf),
            pltpu.VMEM((1, 96), f32),
            pltpu.VMEM((1, 96), f32),
            pltpu.VMEM((2048, 256), bf),
            pltpu.VMEM((1, 256, 256), bf),
            pltpu.VMEM((1, 256), f32),
            pltpu.VMEM((2, 2048, 512), bf),
            pltpu.VMEM((2, 16, ROWS), f32),
            pltpu.VMEM((2, 16, 128), f32),
            pltpu.VMEM((ROWS, 2048), bf),
            pltpu.VMEM((KEY_ROWS, ROWS), bf),
            pltpu.VMEM((HEADS_HERE, ROWS, 128), bf),
            pltpu.VMEM((ROWS + 32, 256), bf),
            pltpu.VMEM((16, KEY_ROWS, 2 * ROWS), bf),
            pltpu.VMEM((HEADS_HERE, ROWS, 128), f32),
            pltpu.VMEM((HEADS_HERE, 128, 2 * ROWS), bf),
            pltpu.VMEM((HEADS_HERE, 128, 2 * ROWS), bf),
            pltpu.VMEM((HEADS_HERE * 128, LATENT), bf),
            pltpu.VMEM((2, ROWS, 512), f32),
            pltpu.VMEM((2, 4, 256, 512), bf),
            pltpu.VMEM((2, 2, 128, 512), bf),
            pltpu.VMEM((4, ROWS, 256), bf),
            pltpu.VMEM((4, ROWS, 256), bf),
        ]
        + sems,
        compiler_params=pltpu.CompilerParams(
            collective_id=0, has_side_effects=True, vmem_limit_bytes=63 * 2**20
        ),
        name="mixer",
    )(*args)


def solution(mesh):
    placed = (
        P("sp", "tp"), P(), P(), P(), P(None, "tp"), P(), P(), P(), P(None, "tp"), P(), P(),
        P(None, "tp"), P("tp", None, None), P("tp"), P("tp", None), P("tp", None),
        P(None, "tp"), P(None, "tp"),
    )
    return jax.shard_map(body, mesh=mesh, in_specs=placed, out_specs=P("sp", "tp"), check_vma=False)
```

time: 238 us -> 77.2 us (0.32)
  waiting for transfers between devices: 105 us -> 0 us
  starting transfers between devices: 26 us -> 0 us
  local copies, waits for them, and re-layouts: 19.7 us -> 1.77 us
  matrix products: 17.8 us -> 0 us
  Pallas kernels: 64.2 us -> 74.2 us
  other arithmetic: 2.97 us -> 0 us
    all_to_all x5 -> x0, waiting for transfers between devices: 104 us -> none  [the longest x1 93.1 us: gathered_copies(): lax.all_to_all(copies, axis, split_axis=0, concat_axis=0, tiled=True)]
    all_to_all x5 -> x0, starting transfers between devices: 21 us -> none  [the longest x1 5.69 us: gathered_copies(): lax.all_to_all(copies, axis, split_axis=0, concat_axis=0, tiled=True)]
    dot_general x6 -> x0, matrix products: 17.8 us -> none  [the longest x1 4.1 us: body(): jnp.dot(normed, w_gate_pool, preferred_element_type=f32)]
    unnamed x31 -> x1, local copies, waits for them, and re-layouts: 12.2 us -> 1.77 us
    pallas_call x2 -> x1, Pallas kernels: 64.2 us -> 74.2 us  [body(): pl.pallas_call(mixer_kernel, out_shape=jax.ShapeDtypeStruct((ROWS, 512),...]
    broadcast_in_dim x1 -> x0, local copies, waits for them, and re-layouts: 5.93 us -> none  [gathered_copies(): copies = jnp.broadcast_to(value, (lax.axis_size(axis), *value.shape))]
    ppermute x2 -> x0, starting transfers between devices: 5.03 us -> none  [the longest x1 3.61 us: extended(): lax.ppermute(tail, 'sp', [(i, (i + 1) % count) for i in range(ends)])]
    concatenate x1 -> x0, other arithmetic: 2.79 us -> none  [body(): jnp.concatenate([w_attn_out, w_pool_out], axis=1)]
  transfers between devices with their start and end apart: 7 -> 0, of which waited for: 5 -> 0; matrix products, arithmetic and copies ran while one was open for 6% -> 0% of each run, Pallas kernels for 0% -> 0%
where the time goes in v2:
time: 77.2 us; the launch traced here: 76 us
  Pallas kernels  74.2 us (96%)
  local copies, waits for them, and re-layouts  1.77 us (2%)
    pallas_call x1, Pallas kernels, body(): pl.pallas_call(mixer_kernel, out_shape=jax.ShapeDtypeStruct((ROWS, 512),...  74.2 us
    unnamed x1, local copies, waits for them, and re-layouts  1.77 us

profile of v2, /device:TPU:0, one launch (start us, length us, event | category | flops | bytes accessed | tf_op | source)
XLA Modules:
  0.0 76.0 jit_solution(17696802877047640399)
XLA Ops:
  0.0 74.2 %mixer.1 = bf16[384,512]{1,0:T(8,128)(2,1)} custom-call(bf16[384,512]{1,0:T(8,128)(2,1)} %tok.1, f32[1,2048]{1,0:T(1,128)} %bitcast.8, bf16[2048,512]{1,0:T(8,128)(2,1)} %wq_h.1, f32[1,512]{1,0:T(1,128)} %bitcast.9, bf16[512,384]{1,0:T(8,128)(2,1)} %wu_h.1, bf16[2048,256]{1,0:T(8,128)(2,1)} %wl_h.1, f32[1,256]{1,0:T(1,128)} %bitcast.10, ...), custom_call_target="tpu_custom_call" | custom-call | tf_op jit(solution)/shard_map/mixer/pallas_call | solution.py:547
  74.2 1.8 %copy.22 = bf16[384,512]{1,0:T(8,128)(2,1)} copy(bf16[384,512]{1,0:T(8,128)(2,1)} %mixer.1) | data formatting | bytes 786432

commit v3 on v2

--- a/solution.py
+++ b/solution.py
@@ -48,6 +48,14 @@
     (3, 2), (1, 2), (2, 3), (2, 1),
     (2, 2),
 )
+EVENTS = (4, 5, 5, 7, 9, 9, 12)
+FULL = 11
+EARLY_GATES = 1
+FILL_GATES = 2
+CODES = tuple(
+    int(np.uint32(sum(off[i] << (2 * k) for k, off in enumerate(ORDER))).astype(np.int32))
+    for i in range(2)
+)
 HALVES = ((0, 160), (160, 144))
 PARTS = (((0, 80), (80, 80)), ((160, 80), (240, 64)))
 STEPS = (1, 3)
@@ -58,7 +66,8 @@
     wao_h, wpo_h, wga_h, wgp_h, fine_h, coarse_h,
     out,
     whole, ng, wq, qg, wu, wl, lg, wr, w_up, qhg, khg, wpi, mix, ps, wg, fine, coarse,
-    normed, block, q, padded, g, acc, kt, vt, wt, gates, w_out, stage, prow, arow,
+    normed, block, q, padded, g, acc, kt_a, vt_a, kt_b, vt_b, wt, gates, part, w_out, stage,
+    prow, arow,
     load_sem, tok_sem, wown_sem, xt, xa, xp, xw, halo, s_across, r_across,
     s_1f, r_1f, s_1h, r_1h, s_2o, r_2o, s_2f, r_2f, s_2h, r_2h, s_d, r_d,
 ):
@@ -114,29 +123,29 @@
             s_across.at[c], r_across.at[c],
         )
 
-    def first_part(half, d):
-        part = region(offsets(half, STEPS[1 - d], 0), PARTS[half][d])
+    def first_part(half, d, c=None):
+        part = region(offsets(half, STEPS[1 - d], 0), PARTS[half][d], c)
         return copy(
             part, part, device(*offsets(half, STEPS[d], 0)),
             s_1h.at[half, d], r_1h.at[half, d],
         )
 
-    def second_full(half, along, d):
-        part = region(offsets(half, along, 0), HALVES[half])
+    def second_full(half, along, d, c=None):
+        part = region(offsets(half, along, 0), HALVES[half], c)
         return copy(
             part, part, device(*offsets(half, 0, STEPS[d])),
             s_2f.at[half, along, d], r_2f.at[half, along, d],
         )
 
-    def second_part(half, along, d):
-        part = region(offsets(half, along, STEPS[1 - d]), PARTS[half][d])
+    def second_part(half, along, d, c=None):
+        part = region(offsets(half, along, STEPS[1 - d]), PARTS[half][d], c)
         return copy(
             part, part, device(*offsets(half, 0, STEPS[d])),
             s_2h.at[half, along, d], r_2h.at[half, along, d],
         )
 
-    def across_chip(half, off):
-        part = region(off, HALVES[half])
+    def across_chip(half, off, c=None):
+        part = region(off, HALVES[half], c)
         at = off[0] * 4 + off[1]
         return copy(part, part, (partner, tp), s_d.at[half, at], r_d.at[half, at])
 
@@ -159,8 +168,8 @@
     def token_copy(kind, c):
         return along_x(whole, pl.multiple_of(c * CHUNK, CHUNK), CHUNK, xt, kind, c)
 
-    def attn_copy(kind, c):
-        return along_x(arow, c * CHUNK, CHUNK, xa, kind, c)
+    def attn_copy(kind, pair, c):
+        return along_x(arow.at[pair], c * CHUNK, CHUNK, xa, kind, pair * CHUNKS + c)
 
     def pool_copy(kind):
         return along_x(prow, 0, ROWS, xp, kind, 0)
@@ -170,17 +179,29 @@
 
     w_src = (wao_h, wpo_h)
 
-    def weight_copy(kind, w):
+    def weight_copy(kind, w=None):
         to = right if kind % 2 == 0 else left
         if kind < 2:
-            src, dst = w_src[w].at[:, columns(to)], w_out.at[w, tp]
+            src = w_src[w or 0].at[:, columns(to)]
+            dst = w_out.at[core, tp]
         elif kind < 4:
-            src = w_src[w].at[pl.ds(128 * (kind - 2), 128), columns(opposite_x)]
-            dst = stage.at[w, kind - 2]
+            src = w_src[w or 0].at[pl.ds(128 * (kind - 2), 128), columns(opposite_x)]
+            dst = stage.at[kind - 2]
+        elif kind < 6:
+            src = stage.at[kind - 4]
+            dst = w_out.at[core, left if kind == 4 else right, pl.ds(128 * (kind - 4), 128)]
         else:
-            src = stage.at[w, kind - 4]
-            dst = w_out.at[w, left if kind == 4 else right, pl.ds(128 * (kind - 4), 128)]
-        return copy(src, dst, (sp, to), xw.at[0, kind, w], xw.at[1, kind, w])
+            src = dst = w_out.at[core, (left, right, opposite_x)[kind - 6]]
+        peer = (sp, to) if kind < 6 else (partner, tp)
+        return copy(src, dst, peer, xw.at[0, kind], xw.at[1, kind])
+
+    def send_weights(kinds):
+        for w in range(2):
+
+            @pl.when(core == w)
+            def _():
+                for kind in kinds:
+                    weight_copy(kind, w).start()
 
     def halo_copy(kind):
         if kind == 0:
@@ -197,8 +218,6 @@
         (mix_h, mix), (ps_h, ps), (wup_h, w_up), (wga_h, wg.at[0]), (wgp_h, wg.at[1]),
     )
     loads = [pltpu.make_async_copy(s, d, load_sem.at[i]) for i, (s, d) in enumerate(pairs)]
-    for load in loads:
-        load.start()
     own_weights = [
         pltpu.make_async_copy(w_src[w].at[:, columns(tp)], w_out.at[w, tp], wown_sem.at[w])
         for w in range(2)
@@ -211,6 +230,8 @@
     for peer in peers:
         pl.semaphore_signal(barrier, inc=1, device_id=peer, device_id_type=MESH)
     own_tokens.wait()
+    for load in loads:
+        load.start()
     pl.semaphore_wait(barrier, len(peers))
 
     for c in range(2):
@@ -231,12 +252,42 @@
     for load in loads[7:]:
         load.wait()
 
+    def neighbours(c):
+        for half in range(2):
+            for d in range(2):
+                own_first(half, d, c).wait_recv()
+                first_part(half, d, c).start()
+        for half in range(2):
+            for d in range(2):
+                own_second(half, d, c).wait_recv()
+                second_part(half, 0, d, c).start()
+        for half in range(2):
+            for d in range(2):
+                across_chip(half, offsets(half, STEPS[1 - d], 0), c).start()
+                across_chip(half, offsets(half, 0, STEPS[1 - d]), c).start()
+        for half in range(2):
+            for d in range(2):
+                for e in range(2):
+                    second_full(half, STEPS[1 - d], e, c).start()
+
+    def gate_rows(c):
+        rows = slice(c * CHUNK, (c + 1) * CHUNK)
+        for k in range(2):
+            gates[k, rows] = jax.nn.sigmoid(
+                jnp.dot(normed[rows, :], wg[k], preferred_element_type=f32)
+            )
+
     def front_step(c, carry):
         @pl.when(c < CHUNKS - 1)
         def _():
             for kind in range(2):
                 token_copy(kind, c + 1).wait_recv()
                 token_copy(kind + 2, c + 1).start()
+
+        @pl.when(c == CHUNKS - 1)
+        def _():
+            for early in range(EARLY_GATES):
+                gate_rows(early)
 
         for kind in range(2):
             token_copy(kind + 2, c).wait_recv()
@@ -301,36 +352,33 @@
         padded[pl.ds(pl.multiple_of(c * CHUNK + 16, 16), CHUNK), :] = jnp.dot(
             here, wpi[...], preferred_element_type=f32
         ).astype(bf)
+
+        @pl.when(c == CHUNKS - 1)
+        def _():
+            neighbours(0)
+
         return carry
 
     lax.fori_loop(0, CHUNKS, front_step, 0)
-    for w in range(2):
-        for kind in (2, 3):
-            weight_copy(kind, w).start()
-    for kind in (0, 1):
-        weight_copy(kind, 0).start()
+    send_weights((2, 3, 0, 1))
     for own in own_weights:
         own.start()
 
     acc[...] = jnp.zeros_like(acc)
-    wt[...] = w_up[...].astype(f32).T.astype(bf)
     for h in range(HEADS_HERE):
-        kt[h, HEAD:128] = jnp.zeros((32, 2 * ROWS), bf)
-        vt[h, VALUE_DIM:128] = jnp.where(
-            lax.broadcasted_iota(jnp.int32, (64, 2 * ROWS), 0) == 0, 1.0, 0.0
-        ).astype(bf)
+        wt[h] = w_up[:, h * 128 : (h + 1) * 128].astype(f32).T.astype(bf)
+    for kt, vt in ((kt_a, vt_a), (kt_b, vt_b)):
+        for h in range(HEADS_HERE):
+            kt[h, HEAD:128] = jnp.zeros((32, 2 * ROWS), bf)
+            vt[h, VALUE_DIM:128] = jnp.where(
+                lax.broadcasted_iota(jnp.int32, (64, 2 * ROWS), 0) == 0, 1.0, 0.0
+            ).astype(bf)
     for kind in range(2):
         halo_copy(kind).start()
     for c in range(CHUNKS):
         own_across(c).wait_recv()
 
-    def gates_and_pool():
-        for k in range(2):
-            for n in range(2):
-                cols = slice(n * 256, (n + 1) * 256)
-                gates[k, :, cols] = jax.nn.sigmoid(
-                    jnp.dot(normed[...], wg[k, :, cols], preferred_element_type=f32)
-                )
+    def pool():
         for kind in range(2):
             halo_copy(kind).wait_recv()
         reach = jnp.where(tp == 0, 1, jnp.where(tp == 1, 2, jnp.where(tp == 2, 4, 8)))
@@ -347,26 +395,6 @@
         grouped = jnp.dot(mixed, mix[0], preferred_element_type=f32)
         prow[tp] = (grouped * ps[...]).astype(bf)
 
-    def neighbours():
-        for half in range(2):
-            for d in range(2):
-                for c in range(CHUNKS):
-                    own_first(half, d, c).wait_recv()
-                first_part(half, d).start()
-        for half in range(2):
-            for d in range(2):
-                for c in range(CHUNKS):
-                    own_second(half, d, c).wait_recv()
-                second_part(half, 0, d).start()
-        for half in range(2):
-            for d in range(2):
-                across_chip(half, offsets(half, STEPS[1 - d], 0)).start()
-                across_chip(half, offsets(half, 0, STEPS[1 - d])).start()
-        for half in range(2):
-            for d in range(2):
-                for e in range(2):
-                    second_full(half, STEPS[1 - d], e).start()
-
     def send_pool():
         for kind in range(2):
             pool_copy(kind).start()
@@ -383,12 +411,15 @@
             across_chip(half, offsets(half, 0, 2)).start()
 
     def pass_weights():
-        for w in range(2):
-            for kind in (2, 3):
-                weight_copy(kind, w).wait_recv()
-                weight_copy(kind + 2, w).start()
-        for kind in (0, 1):
-            weight_copy(kind, 1).start()
+        for kind in (2, 3):
+            weight_copy(kind).wait_recv()
+            weight_copy(kind + 2).start()
+
+    def share_weights():
+        for kind in (0, 1, 4, 5):
+            weight_copy(kind).wait_recv()
+        for kind in (6, 7, 8):
+            weight_copy(kind).start()
 
     def diagonal():
         for half in range(2):
@@ -420,87 +451,147 @@
                 second_part(half, 2, d).wait_recv()
             across_chip(half, (2, 2)).start()
 
-    events = (
-        (1, gates_and_pool), (1, neighbours), (1, send_pool), (3, opposite), (4, pass_weights),
-        (6, diagonal), (8, pass_pool), (9, far), (11, farthest),
-    )
-
-    def chosen(t, values):
-        return sum(jnp.where(t == k, v, 0) for k, v in enumerate(values) if v)
-
-    def step(t, carry):
-        for at, event in events:
-            pl.when(t == at)(event)
-        dy = chosen(t, [o[0] for o in ORDER])
-        dz = chosen(t, [o[1] for o in ORDER])
-
-        @pl.when(t > 0)
-        def _():
-            for half in range(2):
-                arrived_across(half, (dy, dz)).wait_recv()
-
-        at = slot(dy, dz)
+    def finish(pair):
+        for c in range(CHUNKS):
+            rows = slice(c * CHUNK, (c + 1) * CHUNK)
+            for i in range(2):
+                a = acc[2 * pair + i, rows]
+                arow[pair, tp, rows, i * VALUE_DIM : (i + 1) * VALUE_DIM] = (
+                    a[:, 0:VALUE_DIM] / a[:, VALUE_DIM : VALUE_DIM + 1]
+                ).astype(bf)
+
+    def send_rows(pair, c):
+        for kind in range(2):
+            attn_copy(kind, pair, c).start()
+
+    def first_rows():
+        finish(0)
+        for c in range(CHUNKS):
+            send_rows(0, c)
+
+    def pass_rows():
+        for c in range(CHUNKS):
+            for kind in range(2):
+                attn_copy(kind, 0, c).wait_recv()
+                attn_copy(kind + 2, 0, c).start()
+
+    def slot_of(b):
+        return slot(*((code >> (2 * b)) & 3 for code in CODES))
+
+    def landed(b):
+        dy, dz = ((code >> (2 * b)) & 3 for code in CODES)
+        for half in range(2):
+            arrived_across(half, (dy, dz)).wait_recv()
+
+    def prepare(b, heads, kt, vt):
+        at = slot_of(b)
         lat = g[at, 0:LATENT, :]
         rot = g[at, LATENT : LATENT + ROPE, :].astype(f32)
         squares = g[at, LATENT + ROPE : KEY_ROWS, :].astype(f32)
         squares = squares[0:1] + squares[1:2]
-        for h in range(HEADS_HERE):
-            kv = jnp.dot(wt[h * 128 : (h + 1) * 128, :], lat, preferred_element_type=f32)
+        for h in heads:
+            kv = jnp.dot(wt[h], lat, preferred_element_type=f32)
             k = kv[0:NOPE]
             r = lax.rsqrt((jnp.sum(k * k, axis=0, keepdims=True) + squares) * (1.0 / HEAD) + eps)
             kt[h, 0:NOPE] = (k * r).astype(bf)
             kt[h, NOPE:HEAD] = (rot * r).astype(bf)
             vt[h, 0:VALUE_DIM] = kv[NOPE:128].astype(bf)
-        for h in range(HEADS_HERE):
+
+    def attend(heads, kt, vt):
+        for h in heads:
             scores = jnp.dot(q[h], kt[h], preferred_element_type=f32)
             weights = jnp.exp2(scores).astype(bf)
             acc[h] += lax.dot_general(
                 weights, vt[h], (((1,), (1,)), ((), ())), preferred_element_type=f32
             )
-        return carry
-
-    lax.fori_loop(0, 16, step, 0)
-
+
+    every = range(HEADS_HERE)
+    prepare(0, every, kt_a, vt_a)
+    for c in range(EARLY_GATES, FILL_GATES):
+        gate_rows(c)
+    attend(every, kt_a, vt_a)
+    neighbours(1)
+    for c in range(FILL_GATES, CHUNKS):
+        gate_rows(c)
+    neighbours(2)
+    pool()
+    landed(1)
+    send_pool()
+    prepare(1, every, kt_a, vt_a)
+    events = tuple(zip(EVENTS, (
+        opposite, pass_weights, diagonal, pass_pool, share_weights, far, farthest,
+    )))
+
+    def pairs_of_blocks(first, heads, arriving):
+        def step(n, carry):
+            b = 2 * n + first
+            for off, (k_now, v_now, k_next, v_next) in (
+                (1, (kt_a, vt_a, kt_b, vt_b)), (2, (kt_b, vt_b, kt_a, vt_a))
+            ):
+                if arriving:
+                    for at, event in events:
+                        if at in range(first + off, first + 2 * steps + off, 2):
+                            pl.when(b + off == at)(event)
+                    landed(b + off)
+                attend(heads, k_now, v_now)
+                prepare(b + off, heads, k_next, v_next)
+            return carry
+
+        steps = ((FULL if first == 1 else 15) - first) // 2
+        lax.fori_loop(0, steps, step, 0)
+
+    pairs_of_blocks(1, every, True)
+    pairs_of_blocks(FULL, (0, 1), True)
+    attend((0, 1), kt_a, vt_a)
+    first_rows()
+    pairs_of_blocks(FULL, (2, 3), False)
+    attend((2, 3), kt_a, vt_a)
+
+    finish(1)
+    for own in own_weights:
+        own.wait()
+    for kind in (6, 7, 8):
+        there = w_out.at[1 - core, (left, right, opposite_x)[kind - 6]]
+        copy(there, there, (partner, tp), xw.at[0, kind], xw.at[1, kind]).wait_recv()
+    for c in range(CHUNKS):
+        send_rows(1, c)
+    pass_rows()
+    for kind in range(2):
+        pool_copy(kind + 2).wait_recv()
+    gates[1] = gates[1] * sum(
+        jnp.dot(prow[k], w_out[1, k], preferred_element_type=f32) for k in range(4)
+    )
+    for c in range(CHUNKS):
+        for kind in range(2):
+            attn_copy(kind, 1, c).wait_recv()
+            attn_copy(kind + 2, 1, c).start()
+
+    def projected(pair, rows):
+        return sum(
+            jnp.dot(
+                arow[pair, k, rows], w_out[0, k, pair * 128 : (pair + 1) * 128],
+                preferred_element_type=f32,
+            )
+            for k in range(4)
+        )
+
+    for c in range(CHUNKS):
+        for kind in range(2):
+            attn_copy(kind + 2, 0, c).wait_recv()
+    part[...] = projected(0, slice(0, ROWS))
     for c in range(CHUNKS):
         rows = slice(c * CHUNK, (c + 1) * CHUNK)
-        for h in range(HEADS_HERE):
-            a = acc[h, rows]
-            arow[tp, rows, h * VALUE_DIM : (h + 1) * VALUE_DIM] = (
-                a[:, 0:VALUE_DIM] / a[:, VALUE_DIM : VALUE_DIM + 1]
-            ).astype(bf)
-        if c > 0:
-            for kind in range(2):
-                attn_copy(kind, c - 1).start()
-    for own in own_weights:
-        own.wait()
-    for w in range(2):
-        for kind in (0, 1, 4, 5):
-            weight_copy(kind, w).wait_recv()
-    for kind in range(2):
-        attn_copy(kind, CHUNKS - 1).start()
-        pool_copy(kind + 2).wait_recv()
-
-    def projected(buf, rows, w):
-        return sum(
-            jnp.dot(buf[k, rows], w_out[w, k], preferred_element_type=f32) for k in range(4)
-        )
-
-    everything = slice(0, ROWS)
-    gates[1] = gates[1] * projected(prow, everything, 1)
-    for c in range(CHUNKS):
-        for kind in range(2):
-            attn_copy(kind, c).wait_recv()
-            attn_copy(kind + 2, c).start()
-    for c in range(CHUNKS):
-        rows = slice(c * CHUNK, (c + 1) * CHUNK)
-        for kind in range(2):
-            attn_copy(kind + 2, c).wait_recv()
-        out[rows, :] = (gates[0, rows] * projected(arow, rows, 0) + gates[1, rows]).astype(bf)
+        for kind in range(2):
+            attn_copy(kind + 2, 1, c).wait_recv()
+        out[rows, :] = (
+            gates[0, rows] * (part[rows] + projected(1, rows)) + gates[1, rows]
+        ).astype(bf)
 
     for c in range(CHUNKS):
         for kind in range(4):
             token_copy(kind, c).wait_send()
-            attn_copy(kind, c).wait_send()
+            for pair in range(2):
+                attn_copy(kind, pair, c).wait_send()
         own_across(c).wait_send()
         for half in range(2):
             for d in range(2):
@@ -508,9 +599,8 @@
                 own_second(half, d, c).wait_send()
     for kind in range(4):
         pool_copy(kind).wait_send()
-    for w in range(2):
-        for kind in range(6):
-            weight_copy(kind, w).wait_send()
+    for kind in range(9):
+        weight_copy(kind).wait_send()
     for half in range(2):
         halo_copy(half).wait_send()
         for d in range(2):
@@ -540,13 +630,13 @@
         fine, coarse,
     )
     dma = pltpu.SemaphoreType.DMA
-    sems = [dma((17,)), dma((1,)), dma((2,)), dma((2, 4, 3)), dma((2, 4, 3)), dma((2, 4, 1))]
-    sems += [dma((2, 6, 2)), dma((2, 2)), dma((3,)), dma((3,))]
+    sems = [dma((17,)), dma((1,)), dma((2,)), dma((2, 4, 3)), dma((2, 4, 6)), dma((2, 4, 1))]
+    sems += [dma((2, 9)), dma((2, 2)), dma((3,)), dma((3,))]
     for shape in ((2, 2, 3), (2, 2), (2, 2, 3), (2, 4, 2), (2, 4, 2), (2, 16)):
         sems += [dma(shape), dma(shape)]
     return pl.pallas_call(
         mixer_kernel,
-        out_shape=jax.ShapeDtypeStruct((ROWS, 512), bf),
+        out_shape=pltpu.VMEM((ROWS, 512), bf),
         in_specs=[pl.BlockSpec(memory_space=pl.ANY)] * len(args),
         out_specs=pl.BlockSpec(memory_space=pltpu.VMEM),
         scratch_shapes=[
@@ -575,16 +665,19 @@
             pltpu.VMEM((HEADS_HERE, ROWS, 128), f32),
             pltpu.VMEM((HEADS_HERE, 128, 2 * ROWS), bf),
             pltpu.VMEM((HEADS_HERE, 128, 2 * ROWS), bf),
-            pltpu.VMEM((HEADS_HERE * 128, LATENT), bf),
+            pltpu.VMEM((HEADS_HERE, 128, 2 * ROWS), bf),
+            pltpu.VMEM((HEADS_HERE, 128, 2 * ROWS), bf),
+            pltpu.VMEM((HEADS_HERE, 128, LATENT), bf),
             pltpu.VMEM((2, ROWS, 512), f32),
+            pltpu.VMEM((ROWS, 512), f32),
             pltpu.VMEM((2, 4, 256, 512), bf),
-            pltpu.VMEM((2, 2, 128, 512), bf),
+            pltpu.VMEM((2, 128, 512), bf),
             pltpu.VMEM((4, ROWS, 256), bf),
-            pltpu.VMEM((4, ROWS, 256), bf),
+            pltpu.VMEM((2, 4, ROWS, 128), bf),
         ]
         + sems,
         compiler_params=pltpu.CompilerParams(
-            collective_id=0, has_side_effects=True, vmem_limit_bytes=63 * 2**20
+            collective_id=0, has_side_effects=True, vmem_limit_bytes=60 * 2**20
         ),
         name="mixer",
     )(*args)

time: 77.2 us -> 68.4 us (0.89); the launches traced: 76 us -> 68.2 us
  Pallas kernels: 74.2 us -> 67.5 us
  local copies, waits for them, and re-layouts: 1.77 us -> 0.75 us
    pallas_call x1, Pallas kernels: 74.2 us -> 67.5 us  [body(): pl.pallas_call(mixer_kernel, out_shape=pltpu.VMEM((ROWS, 512), bf), in_sp...]
    unnamed x1, local copies, waits for them, and re-layouts: 1.77 us -> 0.75 us
where the time goes in v3:
time: 68.4 us; the launch traced here: 68.2 us
  Pallas kernels  67.5 us (99%)
  local copies, waits for them, and re-layouts  0.75 us (1%)
    pallas_call x1, Pallas kernels, body(): pl.pallas_call(mixer_kernel, out_shape=pltpu.VMEM((ROWS, 512), bf), in_sp...  67.5 us

profile of v3, /device:TPU:0, one launch (start us, length us, event | category | flops | bytes accessed | tf_op | source)
XLA Modules:
  0.0 68.2 jit_solution(1802380371026254804)
XLA Ops:
  0.0 67.5 %mixer.1 = bf16[384,512]{1,0:T(8,128)(2,1)S(1)} custom-call(bf16[384,512]{1,0:T(8,128)(2,1)} %tok.1, f32[1,2048]{1,0:T(1,128)} %bitcast.8, bf16[2048,512]{1,0:T(8,128)(2,1)} %wq_h.1, f32[1,512]{1,0:T(1,128)} %bitcast.9, bf16[512,384]{1,0:T(8,128)(2,1)} %wu_h.1, bf16[2048,256]{1,0:T(8,128)(2,1)} %wl_h.1, f32[1,256]{1,0:T(1,128)} %bitcast.10, ...), custom_call_target="tpu_custom_call" | custom-call | tf_op jit(solution)/shard_map/mixer/pallas_call | solution.py:637
  67.5 0.7 %copy.22 = bf16[384,512]{1,0:T(8,128)(2,1)} copy(bf16[384,512]{1,0:T(8,128)(2,1)S(1)} %mixer.1) | data formatting | bytes 786432

commit v4 on v3

--- a/solution.py
+++ b/solution.py
@@ -50,8 +50,6 @@
 )
 EVENTS = (4, 5, 5, 7, 9, 9, 12)
 FULL = 11
-EARLY_GATES = 1
-FILL_GATES = 2
 CODES = tuple(
     int(np.uint32(sum(off[i] << (2 * k) for k, off in enumerate(ORDER))).astype(np.int32))
     for i in range(2)
@@ -165,8 +163,22 @@
             part = buf.at[right, pl.ds(pl.multiple_of(first + n // 2, 16), n // 2)]
         return copy(part, part, (sp, to), sem.at[0, kind, i], sem.at[1, kind, i])
 
-    def token_copy(kind, c):
-        return along_x(whole, pl.multiple_of(c * CHUNK, CHUNK), CHUNK, xt, kind, c)
+    PIECES = ((0, 128), (128, 128), (256, 64), (320, 64))
+    OF_CHUNK = ((0,), (1,), (2, 3))
+
+    def token_copy(kind, p):
+        return along_x(whole, *PIECES[p], xt, kind, p)
+
+    def relay_tokens(c):
+        for p in OF_CHUNK[c]:
+            for kind in range(2):
+                token_copy(kind, p).wait_recv()
+                token_copy(kind + 2, p).start()
+
+    def all_tokens(c):
+        for p in OF_CHUNK[c]:
+            for kind in range(2):
+                token_copy(kind + 2, p).wait_recv()
 
     def attn_copy(kind, pair, c):
         return along_x(arow.at[pair], c * CHUNK, CHUNK, xa, kind, pair * CHUNKS + c)
@@ -210,8 +222,14 @@
             src, dst, to = padded.at[16:32], padded.at[400:416], (sp + 31) % 32
         return copy(src, dst, (to, tp), halo.at[0, kind], halo.at[1, kind])
 
-    own_tokens = pltpu.make_async_copy(tok, whole.at[tp], tok_sem.at[0])
-    own_tokens.start()
+    own_tokens = [
+        pltpu.make_async_copy(
+            tok.at[pl.ds(c * CHUNK, CHUNK)], whole.at[tp, pl.ds(c * CHUNK, CHUNK)], tok_sem.at[c]
+        )
+        for c in range(CHUNKS)
+    ]
+    for own in own_tokens:
+        own.start()
     pairs = (
         (ng_h, ng), (fine_h, fine), (coarse_h, coarse), (qhg_h, qhg), (khg_h, khg), (lg_h, lg),
         (qg_h, qg), (wl_h, wl), (wr_h, wr), (wq_h, wq), (wu_h, wu), (wpi_h, wpi),
@@ -229,7 +247,7 @@
     peers += [device(*off) for off in ((1, 0), (3, 0), (0, 1), (0, 3))]
     for peer in peers:
         pl.semaphore_signal(barrier, inc=1, device_id=peer, device_id_type=MESH)
-    own_tokens.wait()
+    own_tokens[0].wait()
     for load in loads:
         load.start()
     pl.semaphore_wait(barrier, len(peers))
@@ -237,6 +255,7 @@
     for c in range(2):
         for kind in range(2):
             token_copy(kind, c).start()
+        own_tokens[c + 1].wait()
     for load in loads[:7]:
         load.wait()
     pick = lax.broadcasted_iota(jnp.int32, (16, 128), 1) == sp
@@ -244,11 +263,10 @@
     cs = jnp.sum(jnp.where(pick, coarse[1], 0.0), axis=1, keepdims=True)
     q_gain = column(qhg[...])
     k_gain = column(khg[...])
-    for kind in range(2):
-        token_copy(kind, 0).wait_recv()
-        token_copy(kind + 2, 0).start()
-    for kind in range(2):
-        token_copy(kind, 2).start()
+    relay_tokens(0)
+    for p in OF_CHUNK[2]:
+        for kind in range(2):
+            token_copy(kind, p).start()
     for load in loads[7:]:
         load.wait()
 
@@ -270,27 +288,22 @@
                 for e in range(2):
                     second_full(half, STEPS[1 - d], e, c).start()
 
-    def gate_rows(c):
-        rows = slice(c * CHUNK, (c + 1) * CHUNK)
+    def gate_rows(rows):
         for k in range(2):
             gates[k, rows] = jax.nn.sigmoid(
                 jnp.dot(normed[rows, :], wg[k], preferred_element_type=f32)
             )
 
     def front_step(c, carry):
-        @pl.when(c < CHUNKS - 1)
+        for at in range(CHUNKS - 1):
+            pl.when(c == at)(lambda at=at: relay_tokens(at + 1))
+
+        @pl.when(c > 0)
         def _():
-            for kind in range(2):
-                token_copy(kind, c + 1).wait_recv()
-                token_copy(kind + 2, c + 1).start()
-
-        @pl.when(c == CHUNKS - 1)
-        def _():
-            for early in range(EARLY_GATES):
-                gate_rows(early)
-
-        for kind in range(2):
-            token_copy(kind + 2, c).wait_recv()
+            gate_rows(chunk(c - 1))
+
+        for at in range(CHUNKS):
+            pl.when(c == at)(lambda at=at: all_tokens(at))
         rows = chunk(c)
         squares = jnp.zeros((CHUNK, 1), f32)
         for k in range(4):
@@ -328,17 +341,17 @@
         )
         block[:, rows] = made
         g[slot(0, 0), :, lanes(c)] = made
+        own_across(c).start()
+        for half in range(2):
+            for d in range(2):
+                own_first(half, d, c).start()
+        for half in range(2):
+            for d in range(2):
+                own_second(half, d, c).start()
 
         lat = jnp.dot(here, wq[...], preferred_element_type=f32).astype(bf).astype(f32)
         lat = lat * lax.rsqrt(jnp.mean(lat * lat, axis=1, keepdims=True) + eps) * qg[...]
         raw = jnp.dot(lat.astype(bf), wu[...], preferred_element_type=f32)
-        own_across(c).start()
-        for half in range(2):
-            for d in range(2):
-                own_first(half, d, c).start()
-        for half in range(2):
-            for d in range(2):
-                own_second(half, d, c).start()
         raw = raw.astype(bf).astype(f32).T
         for h in range(HEADS_HERE):
             v = raw[h * HEAD : (h + 1) * HEAD]
@@ -507,12 +520,9 @@
 
     every = range(HEADS_HERE)
     prepare(0, every, kt_a, vt_a)
-    for c in range(EARLY_GATES, FILL_GATES):
-        gate_rows(c)
     attend(every, kt_a, vt_a)
     neighbours(1)
-    for c in range(FILL_GATES, CHUNKS):
-        gate_rows(c)
+    gate_rows(slice(ROWS - CHUNK, ROWS))
     neighbours(2)
     pool()
     landed(1)
@@ -589,7 +599,8 @@
 
     for c in range(CHUNKS):
         for kind in range(4):
-            token_copy(kind, c).wait_send()
+            for p in OF_CHUNK[c]:
+                token_copy(kind, p).wait_send()
             for pair in range(2):
                 attn_copy(kind, pair, c).wait_send()
         own_across(c).wait_send()
@@ -630,7 +641,7 @@
         fine, coarse,
     )
     dma = pltpu.SemaphoreType.DMA
-    sems = [dma((17,)), dma((1,)), dma((2,)), dma((2, 4, 3)), dma((2, 4, 6)), dma((2, 4, 1))]
+    sems = [dma((17,)), dma((3,)), dma((2,)), dma((2, 4, 4)), dma((2, 4, 6)), dma((2, 4, 1))]
     sems += [dma((2, 9)), dma((2, 2)), dma((3,)), dma((3,))]
     for shape in ((2, 2, 3), (2, 2), (2, 2, 3), (2, 4, 2), (2, 4, 2), (2, 16)):
         sems += [dma(shape), dma(shape)]

time: 68.4 us -> 68.4 us (level)
  no operation moved by 1% of the time
where the time goes in v4:
time: 68.4 us; the launch traced here: 68.3 us
  Pallas kernels  67.5 us (99%)
  local copies, waits for them, and re-layouts  0.75 us (1%)
    pallas_call x1, Pallas kernels, body(): pl.pallas_call(mixer_kernel, out_shape=pltpu.VMEM((ROWS, 512), bf), in_sp...  67.5 us

profile of v4, /device:TPU:0, one launch (start us, length us, event | category | flops | bytes accessed | tf_op | source)
XLA Modules:
  0.0 68.3 jit_solution(3437461572968400292)
XLA Ops:
  0.0 67.5 %mixer.1 = bf16[384,512]{1,0:T(8,128)(2,1)S(1)} custom-call(bf16[384,512]{1,0:T(8,128)(2,1)} %tok.1, f32[1,2048]{1,0:T(1,128)} %bitcast.8, bf16[2048,512]{1,0:T(8,128)(2,1)} %wq_h.1, f32[1,512]{1,0:T(1,128)} %bitcast.9, bf16[512,384]{1,0:T(8,128)(2,1)} %wu_h.1, bf16[2048,256]{1,0:T(8,128)(2,1)} %wl_h.1, f32[1,256]{1,0:T(1,128)} %bitcast.10, ...), custom_call_target="tpu_custom_call" | custom-call | tf_op jit(solution)/shard_map/mixer/pallas_call | solution.py:648
  67.5 0.7 %copy.22 = bf16[384,512]{1,0:T(8,128)(2,1)} copy(bf16[384,512]{1,0:T(8,128)(2,1)S(1)} %mixer.1) | data formatting | bytes 786432
